TPU v7x, 512 devices: a whole 4x4x16 slice. The times are simulated.
512 devices in a mesh: ep: 32 (over z, core), tp: 16 (over y, x).
Axes of the slice: x: 4, y: 4, z: 16, core: 2. Of those that a mesh axis runs over, the one named last changes fastest.
Arguments:
- mix_in: bfloat16 [8192, 2048], P('ep'), may hold values from -6 to 6
- mix_gain: float32 [2048], replicated, may hold values from 0.1 to 1.9
- w_in_x: bfloat16 [2048, 2048], P(None, 'tp'), may hold values from -0.125 to 0.125
- w_in_y: bfloat16 [2048, 2048], P(None, 'tp'), may hold values from -0.125 to 0.125
- conv_taps: float32 [4, 2048], P(None, 'tp'), may hold values from -3 to 3
- recur_gate_w: bfloat16 [16, 128, 128], P('tp'), may hold values from -0.5 to 0.5
- input_gate_w: bfloat16 [16, 128, 128], P('tp'), may hold values from -0.5 to 0.5
- decay_logit: float32 [2048], P('tp'), may hold values from 4 to 20
- decay_shift: float32 [8192, 2048], P('ep', 'tp'), may hold values from -2.2 to 0
- moe_in: bfloat16 [8192, 2048], P('ep'), may hold values from -6 to 6
- moe_gain: float32 [2048], replicated, may hold values from 0.1 to 1.9
- routes: int32 [8192, 2], P('ep'), may hold values from 0 to 31, all different within a row; in each aligned block of 256 rows (0 to 255, 256 to 511, ...) at most 32 rows name the same one
- route_weight: float32 [8192, 2], P('ep'), may hold values from 0.1 to 1
- expert_gate: bfloat16 [32, 2048, 2048], P('ep', None, 'tp'), may hold values from -0.125 to 0.125
- expert_up: bfloat16 [32, 2048, 2048], P('ep', None, 'tp'), may hold values from -0.125 to 0.125
- expert_down: bfloat16 [32, 2048, 2048], P('ep', None, 'tp'), may hold values from -0.125 to 0.125
Outputs:
- mixer_out: bfloat16 [8192, 2048], P('ep', 'tp')
- moe_out: bfloat16 [8192, 2048], P('ep', 'tp')
Inputs may be any that keep to these rules, and one draw needn't show every extreme that they name: `routes`: each row names 2 different experts. Among the rows of one index of ep no expert is named more than 32 times, a bound that some block reaches.
All inputs are finite; a program needn't handle non-finite values.
Results may differ from a plain program's by a relative error of at most 0.0095.
Values may be sent and summed in bfloat16 or wider, within the bound.
A program may use at most 64 MiB of HBM per device.

v0:
```python
import jax
import jax.numpy as jnp
from jax import lax
from jax.sharding import PartitionSpec as P

epsilon = 1e-06
lru_scale = 8.0


def from_behind(value, axis, by):
    count = lax.axis_size(axis)
    pairs = [(i, i + by) for i in range(count) if 0 <= i + by < count]
    return lax.ppermute(value, axis, pairs)


def copy_for_each(value, axis):
    count = lax.axis_size(axis)
    return lax.all_to_all(
        jnp.broadcast_to(value[None], (count, *value.shape)), axis, 0, 0, tiled=True
    )


def all_in_one(value, axis):
    leaves = jax.tree.leaves(value)
    sequence = sorted(range(len(leaves)), key=lambda k: -leaves[k].size)
    width = (1, *leaves[sequence[0]].shape)[-1]
    lines = [
        jnp.pad(leaves[k].reshape(-1), (0, -leaves[k].size % width)).reshape(-1, width)
        for k in sequence
    ]
    both, at, found = (copy_for_each(jnp.concatenate(lines), axis), 0, {})
    for k, line in zip(sequence, lines):
        slab = both[:, at : at + len(line)].reshape(len(both), -1)
        found[k] = slab[:, : leaves[k].size].reshape(-1, *leaves[k].shape)
        at += len(line)
    numbers = iter(range(len(leaves)))
    return jax.tree.map(lambda _: found[next(numbers)], value)


def combined_pairwise(pieces, combine):
    while len(jax.tree.leaves(pieces)[0]) > 1:
        pieces = jax.vmap(combine)(
            *(jax.tree.map(lambda part: part[side::2], pieces) for side in (0, 1))
        )
    return jax.tree.map(lambda part: part[0], pieces)


def entering(value, axis, combine, identity):
    count, index = (lax.axis_size(axis), lax.axis_index(axis))
    passed = jnp.arange(count) < index

    def kept(part, zero, own):
        part = jnp.where(
            passed.reshape(-1, *(1 for _ in own.shape)), part, jnp.asarray(zero, own.dtype)
        )
        return part

    pieces = all_in_one(value, axis)
    return combined_pairwise(jax.tree.map(kept, pieces, identity, value), combine)


def norm_rows(rows, gain):
    widened = rows.astype(jnp.float32)
    scaled = widened * lax.rsqrt(jnp.mean(widened * widened, axis=-1, keepdims=True) + epsilon)
    return (scaled * gain[None, :]).astype(jnp.bfloat16)


def link(earlier, later):
    return (earlier[0] * later[0], later[0] * earlier[1] + later[1])


def local(
    mix_in,
    mix_gain,
    w_in_x,
    w_in_y,
    conv_taps,
    recur_gate_w,
    input_gate_w,
    decay_logit,
    decay_shift,
    moe_in,
    moe_gain,
    routes,
    route_weight,
    expert_gate,
    expert_up,
    expert_down,
):
    row_count = mix_in.shape[0]
    width_dev = w_in_x.shape[1]
    heads_dev = recur_gate_w.shape[0]
    block_size = recur_gate_w.shape[1]
    tap_count = conv_taps.shape[0]
    mixer_rows = norm_rows(mix_in, mix_gain)
    x_branch = jnp.dot(mixer_rows, w_in_x, preferred_element_type=jnp.float32).astype(jnp.bfloat16)
    y_branch = jnp.dot(mixer_rows, w_in_y, preferred_element_type=jnp.float32).astype(jnp.bfloat16)
    previous = from_behind(x_branch[row_count - (tap_count - 1) :], "ep", 1)
    padded = jnp.concatenate([previous, x_branch], axis=0)
    conv_sum = jnp.zeros((row_count, width_dev), jnp.float32)
    for tap_index in range(tap_count):
        conv_sum = conv_sum + conv_taps[tap_index][None, :] * padded[
            tap_index : tap_index + row_count
        ].astype(jnp.float32)
    x_conv = conv_sum.astype(jnp.bfloat16)
    heads_in = x_conv.reshape(row_count, heads_dev, block_size)
    gate_a = jnp.einsum(
        "thi,hij->thj", heads_in, recur_gate_w, preferred_element_type=jnp.float32
    ).reshape(row_count, width_dev)
    gate_x = jnp.einsum(
        "thi,hij->thj", heads_in, input_gate_w, preferred_element_type=jnp.float32
    ).reshape(row_count, width_dev)
    log_decay = (
        -lru_scale * jax.nn.sigmoid(gate_a) * jax.nn.softplus(-decay_logit)[None, :] + decay_shift
    )
    lru_drive = (
        jnp.sqrt(-jnp.expm1(2.0 * log_decay)) * jax.nn.sigmoid(gate_x) * x_conv.astype(jnp.float32)
    )
    through, local_state = lax.associative_scan(link, (jnp.exp(log_decay), lru_drive), axis=0)
    identity = (jnp.ones((width_dev,), jnp.float32), jnp.zeros((width_dev,), jnp.float32))
    carried = entering((through[row_count - 1], local_state[row_count - 1]), "ep", link, identity)
    lru_state = local_state + through * carried[1][None, :]
    mixer_out = (lru_state * jax.nn.gelu(y_branch.astype(jnp.float32))).astype(jnp.bfloat16)
    moe_rows = norm_rows(moe_in, moe_gain)
    token_count = moe_rows.shape[0]
    feature_count = moe_rows.shape[1]
    choose_count = routes.shape[1]
    expert_count = lax.axis_size("ep")
    capacity = 2 * token_count * choose_count // expert_count
    slot_total = expert_count * capacity
    expert_ids = routes.reshape(-1)
    onehot = (expert_ids[:, None] == jnp.arange(expert_count, dtype=jnp.int32)[None, :]).astype(
        jnp.int32
    )
    slot_rank = jnp.sum(jnp.cumsum(onehot, axis=0) * onehot, axis=1) - 1
    slot_index = expert_ids * capacity + slot_rank
    token_index = jnp.repeat(jnp.arange(token_count, dtype=jnp.int32), choose_count)
    slot_owner = jnp.full((slot_total,), token_count, jnp.int32).at[slot_index].set(token_index)
    padded_rows = jnp.concatenate([moe_rows, jnp.zeros((1, feature_count), jnp.bfloat16)], axis=0)
    outgoing = padded_rows[slot_owner].reshape(expert_count, capacity, feature_count)
    column_width = feature_count // lax.axis_size("tp")
    own_columns = lax.dynamic_slice_in_dim(
        outgoing, lax.axis_index("tp") * column_width, column_width, 2
    )
    incoming = lax.all_to_all(own_columns, "ep", split_axis=0, concat_axis=0, tiled=True)
    piece = lax.all_gather(incoming, "tp", axis=2, tiled=True)
    flat_rows = piece.reshape(slot_total, piece.shape[2])
    gate_rows = expert_gate[0]
    up_rows = expert_up[0]
    gate_proj = jnp.dot(flat_rows, gate_rows, preferred_element_type=jnp.float32)
    up_proj = jnp.dot(flat_rows, up_rows, preferred_element_type=jnp.float32)
    hidden = (jax.nn.silu(gate_proj) * up_proj).astype(jnp.bfloat16)
    down_rows = expert_down[0]
    columns = jnp.dot(
        lax.all_gather(hidden, "tp", axis=1, tiled=True),
        down_rows,
        preferred_element_type=jnp.float32,
    )
    results = columns.astype(jnp.bfloat16).reshape(expert_count, capacity, expert_down.shape[2])
    returned = lax.all_to_all(results, "ep", split_axis=0, concat_axis=0, tiled=True).reshape(
        slot_total, expert_down.shape[2]
    )
    picked = (
        returned[slot_index]
        .astype(jnp.float32)
        .reshape(token_count, choose_count, expert_down.shape[2])
    )
    route_share = route_weight / jnp.sum(route_weight, axis=1, keepdims=True)
    moe_out = jnp.sum(route_share[:, :, None] * picked, axis=1).astype(jnp.bfloat16)
    return (mixer_out, moe_out)


def solution(mesh):
    placed = (
        P("ep", None),
        P(),
        P(None, "tp"),
        P(None, "tp"),
        P(None, "tp"),
        P("tp", None, None),
        P("tp", None, None),
        P("tp"),
        P("ep", "tp"),
        P("ep", None),
        P(),
        P("ep", None),
        P("ep", None),
        P("ep", None, "tp"),
        P("ep", None, "tp"),
        P("ep", None, "tp"),
    )
    return jax.shard_map(
        local, mesh=mesh, in_specs=placed, out_specs=(P("ep", "tp"), P("ep", "tp")), check_vma=False
    )
```

profile of v0, /device:TPU:1, one launch (start us, length us, event | category | flops | bytes accessed | tf_op | source)
XLA Modules:
  0.0 251.2 jit_solution(5826928221437767677)
XLA Ops:
  7.2 0.0 copy-start
  7.2 0.0 copy-start.2
  7.2 0.0 all-gather.3.cloned.1.call-start
  7.3 0.9 copy.27
  8.2 0.1 eq.29
  8.3 0.1 eq.25
  8.5 0.7 broadcast_multiply_fusion
  9.2 1.2 reduce-window.6
  10.3 0.2 slice_reduce_fusion
  10.6 0.1 fusion.43
  10.7 0.1 copy.26
  10.9 0.1 mul.375
  11.0 0.1 reshape.156
  11.2 2.4 scatter_custom_fusion
  13.6 1.5 fusion.3
  15.2 0.3 fusion.5
  15.5 0.1 concatenate.67
  15.6 0.0 copy-start.3
  15.6 6.0 %gather_fusion = bf16[1024,2048]{1,0:T(8,128)(2,1)} fusion(bf16[257,2048]{1,0:T(8,128)(2,1)S(1)} %concatenate.67, s32[1024]{0:T(1024)S(1)} %fusion.51), kind=kCustom, calls=%fused_computation | custom fusion | bytes 8392704 | tf_op jit(solution)/shard_map/gather | solution.py:140
  21.6 1.0 constant_dynamic-slice_fusion
  22.6 0.0 copy-start.5
  22.6 38.9 %all_to_all.15 = bf16[32,32,128]{2,1,0:T(8,128)(2,1)} all-to-all(bf16[32,32,128]{2,1,0:T(8,128)(2,1)S(1)} %constant_dynamic-slice_fusion), channel_id=1, replica_groups=mesh['ep'=32,'tp'=16] {'ep'}, dimensions={0} | all-to-all | bytes 524288 | tf_op jit(solution)/shard_map/all_to_all | solution.py:145
  61.5 0.0 all-gather.3.cloned.1.call-update
  61.5 0.0 all-gather.5.cloned.1.call-start
  61.6 0.3 fusion
  61.9 0.5 convolution_convert_fusion.2
  62.4 2.2 collective-permute-start
  64.7 59.1 %all-gather.3.cloned.1.call-done = bf16[32,32,2048]{2,1,0:T(8,128)(2,1)} async-done(((bf16[32,32,128]{2,1,0:T(8,128)(2,1)}), bf16[32,32,2048]{2,1,0:T(8,128)(2,1)}) %all-gather.3.cloned.1.call-update) | async-done | bytes 4194320 | tf_op jit(solution)/shard_map/all_gather | solution.py:146
  123.8 3.6 %fusion.20 = f32[1024,128]{1,0:T(8,128)S(1)} fusion(bf16[1024,2048]{1,0:T(8,128)(2,1)} %bitcast.61, bf16[1,2048,128]{2,1,0:T(8,128)(2,1)S(1)} %copy-done), kind=kOutput, calls=%fused_computation.33 | convolution fusion | flops 536870912 | bytes 5242880 | tf_op jit(solution)/shard_map/dot_general | solution.py:150
  127.4 0.0 copy-start.15
  127.4 0.0 copy-start.11
  127.4 2.0 fusion.6
  129.4 0.0 all-gather.5.cloned.1.call-update
  129.5 0.1 add_convert_fusion
  129.6 0.2 fusion.61
  129.8 0.2 fusion.16
  132.0 0.6 broadcast_in_dim.27
  132.6 14.4 %all-to-all-start = ((f32[32,2,128]{2,1,0:T(2,128)}), f32[32,2,128]{2,1,0:T(2,128)S(1)}, u32[]{:S(2)}, u32[]{:S(2)}) async-start(f32[32,2,128]{2,1,0:T(2,128)} %broadcast_in_dim.27), calls=%async_computation | async-start | bytes 65536 | tf_op jit(solution)/shard_map/all_to_all | solution.py:18
  147.0 0.1 copy.25
  147.2 11.9 %all-to-all-done = f32[32,2,128]{2,1,0:T(2,128)S(1)} async-done(((f32[32,2,128]{2,1,0:T(2,128)}), f32[32,2,128]{2,1,0:T(2,128)S(1)}, u32[]{:S(2)}, u32[]{:S(2)}) %all-to-all-start) | async-done | bytes 32800 | tf_op jit(solution)/shard_map/all_to_all | solution.py:18
  159.1 0.1 broadcast_select_fusion.1
  159.3 41.9 %all-gather.5.cloned.1.call-done = bf16[1024,2048]{1,0:T(8,128)(2,1)} async-done(((bf16[1024,128]{1,0:T(8,128)(2,1)}), bf16[1024,2048]{1,0:T(8,128)(2,1)}) %all-gather.5.cloned.1.call-update) | async-done | bytes 4194320 | tf_op jit(solution)/shard_map/all_gather | solution.py:155
  201.2 4.1 %convolution_convert_fusion = bf16[1024,128]{1,0:T(8,128)(2,1)} fusion(bf16[1024,2048]{1,0:T(8,128)(2,1)} %all-gather.5.cloned.1.call-done, bf16[1,2048,128]{2,1,0:T(8,128)(2,1)S(1)} %copy-done.9), kind=kOutput, calls=%fused_computation.15 | convolution fusion | flops 537001984 | bytes 4980736 | tf_op jit(solution)/shard_map/dot_general | solution.py:154
  205.3 14.4 %all-to-all-start.2 = ((bf16[32,32,128]{2,1,0:T(8,128)(2,1)}), bf16[32,32,128]{2,1,0:T(8,128)(2,1)S(1)}, u32[]{:S(2)}, u32[]{:S(2)}) async-start(bf16[32,32,128]{2,1,0:T(8,128)(2,1)} %bitcast.17), calls=%async_computation.2 | async-start | bytes 524288 | tf_op jit(solution)/shard_map/all_to_all | solution.py:160
  220.0 1.1 fusion.37
  221.1 20.9 %all-to-all-done.2 = bf16[32,32,128]{2,1,0:T(8,128)(2,1)S(1)} async-done(((bf16[32,32,128]{2,1,0:T(8,128)(2,1)}), bf16[32,32,128]{2,1,0:T(8,128)(2,1)S(1)}, u32[]{:S(2)}, u32[]{:S(2)}) %all-to-all-start.2) | async-done | bytes 262176 | tf_op jit(solution)/shard_map/all_to_all | solution.py:160
  242.0 1.3 gather_fusion.1
  243.3 1.1 fusion.24
  (190 shorter events, 1.8 us)
Async XLA Ops:
  7.2 116.6 %copy-start = (bf16[1,2048,128]{2,1,0:T(8,128)(2,1)S(1)}, bf16[1,2048,128]{2,1,0:T(8,128)(2,1)}, u32[]{:S(2)}) copy-start(bf16[1,2048,128]{2,1,0:T(8,128)(2,1)} %param.29) | copy-start | bytes 1572868
  7.2 8.0 %copy-start.2 = (bf16[256,2048]{1,0:T(8,128)(2,1)S(1)}, bf16[256,2048]{1,0:T(8,128)(2,1)}, u32[]{:S(2)}) copy-start(bf16[256,2048]{1,0:T(8,128)(2,1)} %param.25) | copy-start | bytes 3145732
  7.2 8.0 %copy-start.4 = (f32[2048]{0:T(1024)S(1)}, f32[2048]{0:T(1024)}, u32[]{:S(2)}) copy-start(f32[2048]{0:T(1024)} %param.26) | copy-start | bytes 24580
  7.2 116.6 %all-gather.3.cloned.1.call-start = ((), (), s32[]{:S(2)}) async-start(), calls=%async_computation.3 | async-start | bytes 4456448 | tf_op jit(solution)/shard_map/all_gather | solution.py:146
  15.6 46.0 %copy-start.3 = (bf16[256,2048]{1,0:T(8,128)(2,1)S(1)}, bf16[256,2048]{1,0:T(8,128)(2,1)}, u32[]{:S(2)}) copy-start(bf16[256,2048]{1,0:T(8,128)(2,1)} %param.16) | copy-start | bytes 3145732
  21.6 40.3 %copy-start.7 = (bf16[2048,128]{1,0:T(8,128)(2,1)S(1)}, bf16[2048,128]{1,0:T(8,128)(2,1)}, u32[]{:S(2)}) copy-start(bf16[2048,128]{1,0:T(8,128)(2,1)} %param.18) | copy-start | bytes 1572868
  21.6 40.3 %copy-start.14 = (f32[2048]{0:T(1024)S(1)}, f32[2048]{0:T(1024)}, u32[]{:S(2)}) copy-start(f32[2048]{0:T(1024)} %param.17) | copy-start | bytes 24580
  22.6 42.1 %copy-start.5 = (f32[256,2]{0,1:T(2,128)S(1)}, f32[256,2]{0,1:T(2,128)}, u32[]{:S(2)}) copy-start(f32[256,2]{0,1:T(2,128)} %param.28) | copy-start | bytes 6148
  61.5 139.6 %all-gather.5.cloned.1.call-start = ((), (), s32[]{:S(2)}) async-start(), calls=%async_computation.4 | async-start | bytes 4456448 | tf_op jit(solution)/shard_map/all_gather | solution.py:155
  62.4 67.1 %collective-permute-start = (bf16[3,128]{1,0:T(4,128)(2,1)S(1)}, bf16[3,128]{1,0:T(4,128)(2,1)S(1)}, u32[]{:S(2)}, u32[]{:S(2)}) collective-permute-start(bf16[3,128]{1,0:T(4,128)(2,1)S(1)} %slice.443), channel_id=1, source_target_pairs={{0,16},{16,32},{32,48},{48,64},{64,80},{80,96},{96,112},{112,128},... | collective-permute-start | bytes 2312 | tf_op jit(solution)/shard_map/ppermute | solution.py:13
  123.8 3.6 %copy-start.1 = (bf16[32,32,2048]{2,1,0:T(8,128)(2,1)S(1)}, bf16[32,32,2048]{2,1,0:T(8,128)(2,1)}, u32[]{:S(2)}) copy-start(bf16[32,32,2048]{2,1,0:T(8,128)(2,1)} %all-gather.3.cloned.1.call-done) | copy-start | bytes 12582916
  123.8 3.6 %copy-start.8 = (bf16[1,2048,128]{2,1,0:T(8,128)(2,1)S(1)}, bf16[1,2048,128]{2,1,0:T(8,128)(2,1)}, u32[]{:S(2)}) copy-start(bf16[1,2048,128]{2,1,0:T(8,128)(2,1)} %param.30) | copy-start | bytes 1572868
  127.4 2.1 copy-start.6
  127.4 2.1 copy-start.15
  127.4 2.2 copy-start.11
  127.4 2.2 copy-start.12
  127.4 2.4 copy-start.13
  131.3 69.8 %copy-start.9 = (bf16[1,2048,128]{2,1,0:T(8,128)(2,1)S(1)}, bf16[1,2048,128]{2,1,0:T(8,128)(2,1)}, u32[]{:S(2)}) copy-start(bf16[1,2048,128]{2,1,0:T(8,128)(2,1)} %param.31) | copy-start | bytes 1572868
  132.6 26.4 %all-to-all-start = ((f32[32,2,128]{2,1,0:T(2,128)}), f32[32,2,128]{2,1,0:T(2,128)S(1)}, u32[]{:S(2)}, u32[]{:S(2)}) async-start(f32[32,2,128]{2,1,0:T(2,128)} %broadcast_in_dim.27), calls=%async_computation | async-start | bytes 65536 | tf_op jit(solution)/shard_map/all_to_all | solution.py:18
  159.3 60.7 %copy-start.10 = (bf16[2048,128]{1,0:T(8,128)(2,1)S(1)}, bf16[2048,128]{1,0:T(8,128)(2,1)}, u32[]{:S(2)}) copy-start(bf16[2048,128]{1,0:T(8,128)(2,1)} %param.19) | copy-start | bytes 1572868
  205.3 36.6 %all-to-all-start.2 = ((bf16[32,32,128]{2,1,0:T(8,128)(2,1)}), bf16[32,32,128]{2,1,0:T(8,128)(2,1)S(1)}, u32[]{:S(2)}, u32[]{:S(2)}) async-start(bf16[32,32,128]{2,1,0:T(8,128)(2,1)} %bitcast.17), calls=%async_computation.2 | async-start | bytes 524288 | tf_op jit(solution)/shard_map/all_to_all | solution.py:160
Sparse Core Ops, SparseCore 0:
  61.7 62.0 all-gather.2
  129.6 71.5 all-gather.4
where the time goes:
time: 252 us; the launch traced here: 251 us
  waiting for transfers between devices  134 us (53%)
  blocking collectives  38.9 us (15%)
  starting transfers between devices  31.1 us (12%)
  between operations  15.2 us (6%)
  local copies, waits for them, and re-layouts  14.7 us (6%)
  matrix products  11.7 us (5%)
  other arithmetic  5.83 us (2%)
    all_gather x1, waiting for transfers between devices, local(): piece = lax.all_gather(incoming, 'tp', axis=2, tiled=True)  59.1 us
    all_gather x1, waiting for transfers between devices, local(): lax.all_gather(hidden, 'tp', axis=1, tiled=True)  41.9 us
    all_to_all x1, blocking collectives, local(): lax.all_to_all(own_columns, 'ep', split_axis=0, concat_axis=0, tiled=True)  38.9 us
    all_to_all x1, waiting for transfers between devices, local(): lax.all_to_all(results, 'ep', split_axis=0, concat_axis=0, tiled=True)  20.9 us
    all_to_all x1, starting transfers between devices, copy_for_each(): lax.all_to_all(jnp.broadcast_to(value[None], (count, *value.shape)), axis...  14.4 us
    all_to_all x1, starting transfers between devices, local(): lax.all_to_all(results, 'ep', split_axis=0, concat_axis=0, tiled=True)  14.4 us
    all_to_all x1, waiting for transfers between devices, copy_for_each(): lax.all_to_all(jnp.broadcast_to(value[None], (count, *value.shape)), axis...  11.9 us
    gather x1, local copies, waits for them, and re-layouts, local(): padded_rows[slot_owner].reshape(expert_count, capacity, feature_count)  5.97 us
  transfers between devices with their start and end apart: 5, of which 4 were waited for; matrix products, arithmetic and copies ran while one was open for 4% of the time, Pallas kernels for 0%

commit v1 on v0

v1 whole, which is shorter than its diff:
```python
import functools

import jax
import jax.numpy as jnp
from jax import lax
from jax.experimental import pallas as pl
from jax.experimental.pallas import tpu as pltpu
from jax.sharding import PartitionSpec as P

MESH = pl.DeviceIdType.MESH
F32 = jnp.float32
BF16 = jnp.bfloat16
epsilon = 1e-06
lru_scale = 8.0

RING = 16
CORES = 2
EP = RING * CORES
SIDE = 4
ROWS = 256
D = 2048
LANE = 128
CAP = 32
SLOTS = EP * CAP
CHUNKS = 4
CH = SLOTS // CHUNKS
HALF = CH // 2
QUARTER = HALF // 2

NEAR = [0] + [s * d if s * d > -RING // 2 else RING // 2 for d in range(1, RING // 2 + 1) for s in (1, -1)][: RING - 1]
PLACE = {off % RING: at for at, off in enumerate(NEAR)}

ORDER = [
    ("R1", 0), ("mixA", 0), ("R2", 0), ("R1", 1), ("R3", 0), ("R2", 1), ("R1", 2), ("mixB", 0),
    ("R4", 0), ("R3", 1), ("R2", 2), ("R1", 3), ("mixC", 0), ("up", 0), ("H1", 0),
    ("R4", 1), ("R3", 2), ("R2", 3), ("H2", 0), ("up", 1), ("H1", 1),
    ("R4", 2), ("R3", 3), ("H3", 0), ("H2", 1), ("up", 2), ("H1", 2),
    ("R4", 3), ("H4", 0), ("H3", 1), ("H2", 2), ("up", 3), ("H1", 3), ("mixD", 0),
    ("down", 0), ("H4", 1), ("H3", 2), ("H2", 3),
    ("down", 1), ("H4", 2), ("H3", 3), ("down", 2), ("H4", 3), ("down", 3),
]


def softplus(v):
    e = jnp.exp(-jnp.abs(v))
    series = e * (1.0 - e * (1.0 / 2 - e * (1.0 / 3 - e * (1.0 / 4 - e * (1.0 / 5 - e / 6)))))
    return jnp.maximum(v, 0.0) + jnp.where(e < 0.03, series, jnp.log(1.0 + e))


def one_minus_exp(v):
    series = 1.0 + v / 8
    for n in (7, 6, 5, 4, 3, 2):
        series = 1.0 + v / n * series
    return jnp.where(v > -0.25, -v * series, 1.0 - jnp.exp(v))


def kernel(
    mix_in, moe_in, w_x, w_y, shift, w_gate, w_up, w_down,
    mix_gain, conv_taps, recur_w, input_w, logit, moe_gain, routes, weight,
    mixer_out, moe_out,
    mix_v, moe_v, win_v, shift_v, gu_v, down_v,
    c0, c1, sent, X, H, res, ret, ybr, xb, xcv, halo_out, halo_in, sa, sb, carry_out, carry_in,
    load_sem, ag_send, ag_recv, d_send, d_recv, r_send, r_recv, k_send, k_recv, h_sem,
):
    ep, tp = lax.axis_index("ep"), lax.axis_index("tp")
    z, core = ep // CORES, lax.rem(ep, CORES)
    y, x = tp // SIDE, lax.rem(tp, SIDE)

    def wrap(v, n):
        return lax.rem(v + 2 * n, n)

    east, west = wrap(x + 1, SIDE), wrap(x - 1, SIDE)
    north, south = wrap(y + 1, SIDE), wrap(y - 1, SIDE)
    plane = [(ep, y * SIDE + east), (ep, y * SIDE + west), (ep, north * SIDE + x), (ep, south * SIDE + x)]

    def peer(at, c):
        return wrap(z + NEAR[at], RING) * CORES + c

    loads = []
    for n, (src, dst) in enumerate([
        (moe_in, moe_v), (mix_in, mix_v), (w_x, win_v.at[:, :LANE]), (w_y, win_v.at[:, LANE:]), (shift, shift_v),
        (w_gate.at[0], gu_v.at[:, :LANE]), (w_up.at[0], gu_v.at[:, LANE:]), (w_down.at[0], down_v),
    ]):
        loads.append(pltpu.make_async_copy(src, dst, load_sem.at[n]))
        loads[-1].start()

    barrier = pltpu.get_barrier_semaphore()

    def greet(where):
        pl.semaphore_signal(barrier, inc=1, device_id=where, device_id_type=MESH)

    for where in plane:
        greet(where)
    greet((peer(0, 1 - core), tp))
    for at in range(1, RING):
        for c in range(CORES):
            greet((peer(at, c), tp))

    pending = []

    def launch(src, dst, ss, rs, where):
        copy = pltpu.make_async_remote_copy(
            src_ref=src, dst_ref=dst, send_sem=ss, recv_sem=rs, device_id=where, device_id_type=MESH
        )
        copy.start()
        pending.append(copy)
        return copy

    def normed(ref, gain, lanes):
        v = ref[...].astype(F32)
        scale = lax.rsqrt(jnp.sum(v * v, axis=1, keepdims=True) / D + epsilon)
        if lanes is not None:
            v = ref[:, lanes].astype(F32)
            return (v * scale * gain[:, lanes]).astype(BF16)
        return (v * scale * gain[...]).astype(BF16)

    lane_e = lax.broadcasted_iota(jnp.int32, (ROWS, LANE), 1)
    onehot = [jnp.where(routes[:, k : k + 1] == lane_e, 1.0, 0.0).astype(BF16) for k in range(2)]
    before = jnp.where(
        lax.broadcasted_iota(jnp.int32, (ROWS, ROWS), 1) < lax.broadcasted_iota(jnp.int32, (ROWS, ROWS), 0), 1.0, 0.0
    ).astype(BF16)
    rank = [jnp.dot(before, hot, preferred_element_type=F32) for hot in onehot]
    rank[1] = rank[1] + jnp.sum(onehot[0].astype(F32), axis=0, keepdims=True)
    lane_1 = lax.broadcasted_iota(jnp.int32, (1, LANE), 1)
    off = (lane_1 // CORES - z + 2 * RING) % RING
    at = jnp.where(off == 0, 0, jnp.where(off <= RING // 2, 2 * off - 1, 2 * (RING - off)))
    base = (CAP * (CORES * at + lane_1 % CORES)).astype(F32)
    slot_lane = lax.broadcasted_iota(jnp.int32, (ROWS, SLOTS), 1)
    for ref, hot, r in zip((c0, c1), onehot, rank):
        slot = jnp.sum(hot.astype(F32) * (r + base), axis=1, keepdims=True).astype(jnp.int32)
        ref[...] = jnp.where(slot_lane == slot, 1.0, 0.0).astype(BF16)

    loads[0].wait()
    own_lanes = pl.ds(pl.multiple_of(tp * LANE, LANE), LANE)
    own_rows = normed(moe_v, moe_gain, own_lanes)
    sent[...] = lax.dot_general(
        c0[...] + c1[...], own_rows, (((0,), (0,)), ((), ())), preferred_element_type=F32
    ).astype(BF16).reshape(EP, CAP, LANE)

    pl.semaphore_wait(barrier, len(plane) + EP - 1)

    def block(buf, p):
        return buf.at[y, x, pl.ds(pl.multiple_of(p * CAP, CAP), CAP)]

    def dispatch(at, c, where):
        place = PLACE[-NEAR[at] % RING] * CORES + core
        launch(sent.at[CORES * at + c], block(X, place), d_send.at[CORES * at + c], d_recv.at[place], (where, tp))

    dispatch(0, 1 - core, peer(0, 1 - core))
    for at in range(1, RING):
        for c in range(CORES):
            dispatch(at, c, peer(at, c))
    own = pl.ds(pl.multiple_of(core * CAP, CAP), CAP)
    X[y, x, own, :] = sent[core]

    def arrived(p, sem, buf_block):
        pltpu.make_async_remote_copy(
            src_ref=buf_block, dst_ref=buf_block, send_sem=sem.at[p], recv_sem=sem.at[p],
            device_id=(ep, tp), device_id_type=MESH,
        ).wait_recv()

    def await_dispatch(k):
        for p in range(k * CH // CAP, (k + 1) * CH // CAP):
            if p < CORES:
                if p == 0:
                    arrived(1 - core, d_recv, block(X, 1 - core))
            else:
                arrived(p, d_recv, block(X, p))

    bufs = {"R": X, "H": H}
    ways = {}

    def gather(kind, step, k):
        buf = bufs[kind]
        lo = k * CH
        xs, ys = pl.ds(lo, HALF), pl.ds(lo + HALF, HALF)
        xa, xz = pl.ds(lo, QUARTER), pl.ds(lo + QUARTER, QUARTER)
        ya, yz = pl.ds(lo + HALF, QUARTER), pl.ds(lo + HALF + QUARTER, QUARTER)
        if step == 1:
            if kind == "R":
                await_dispatch(k)
            views = [buf.at[y, x, xs], buf.at[y, x, xs], buf.at[y, x, ys], buf.at[y, x, ys]]
        elif step == 2:
            views = [buf.at[y, west, xa], buf.at[y, east, xz], buf.at[south, x, ya], buf.at[north, x, yz]]
        elif step == 3:
            views = [buf.at[:, x, ys], buf.at[:, x, ys], buf.at[y, :, xs], buf.at[y, :, xs]]
        else:
            views = [buf.at[:, west, ya], buf.at[:, east, yz], buf.at[south, :, xa], buf.at[north, :, xz]]
        if step == 3:
            for n in range(4):
                ways[kind, 2, k, n].wait_recv()
        for n in range(4):
            if step == 2 or step == 4:
                ways[kind, step - 1, k, n].wait_recv()
            slot = (("RH".index(kind) * CHUNKS + k) * 4 + step - 1) * 4 + n
            ways[kind, step, k, n] = launch(views[n], views[n], ag_send.at[slot], ag_recv.at[slot], plane[n])

    def all_blocks(buf, k):
        rows = pl.ds(k * CH, CH)
        return jnp.concatenate([buf[a, b, rows, :] for a in range(SIDE) for b in range(SIDE)], axis=1)

    def run_up(k):
        for n in range(4):
            ways["R", 4, k, n].wait_recv()
        if k == 0:
            loads[5].wait()
            loads[6].wait()
        both = jnp.dot(all_blocks(X, k), gu_v[...], preferred_element_type=F32)
        g, u = both[:, :LANE], both[:, LANE:]
        H[y, x, pl.ds(k * CH, CH), :] = (g * jax.nn.sigmoid(g) * u).astype(BF16)

    def run_down(k):
        for n in range(4):
            ways["H", 4, k, n].wait_recv()
        if k == 0:
            loads[7].wait()
        out = jnp.dot(all_blocks(H, k), down_v[...], preferred_element_type=F32).astype(BF16)
        first = k * CH // CAP
        res[pl.ds(first, CH // CAP)] = out.reshape(CH // CAP, CAP, LANE)

        def give(at, c, where):
            place = PLACE[-NEAR[at] % RING] * CORES + core
            launch(res.at[CORES * at + c], ret.at[place], r_send.at[CORES * at + c], r_recv.at[place], (where, tp))

        for p in range(first, first + CH // CAP):
            at, c = p // CORES, p % CORES
            if at == 0:
                if c == 0:
                    give(0, 1 - core, peer(0, 1 - core))
                    ret[core] = res[core]
            else:
                give(at, c, peer(at, c))

    def mix_a():
        loads[1].wait()
        loads[2].wait()
        loads[3].wait()
        rows = normed(mix_v, mix_gain, None)
        both = jnp.dot(rows, win_v[...], preferred_element_type=F32).astype(BF16)
        ybr[...] = both[:, LANE:]
        xb[pl.ds(8, ROWS), :] = both[:, :LANE].astype(F32)
        halo_out[...] = both[ROWS - 16 :, :LANE]
        ways["halo"] = launch(halo_out, halo_in, h_sem.at[0], h_sem.at[1], (wrap(ep + 1, EP), tp))

    def mix_b():
        ways["halo"].wait_recv()
        xb[pl.ds(0, 8), :] = jnp.where(ep > 0, halo_in[...].astype(F32)[8:], 0.0)
        conv = jnp.zeros((ROWS, LANE), F32)
        for k in range(4):
            conv = conv + conv_taps[k : k + 1, :] * xb[pl.ds(5 + k, ROWS), :]
        x_conv = conv.astype(BF16)
        xcv[...] = x_conv
        gate_a = jnp.dot(x_conv, recur_w[0], preferred_element_type=F32)
        gate_x = jnp.dot(x_conv, input_w[0], preferred_element_type=F32)
        loads[4].wait()
        log_decay = -lru_scale * jax.nn.sigmoid(gate_a) * softplus(-logit[...]) + shift_v[...]
        sa[...] = jnp.exp(log_decay)
        sb[...] = jnp.sqrt(one_minus_exp(2.0 * log_decay)) * jax.nn.sigmoid(gate_x) * x_conv.astype(F32)

    def mix_c():
        a, b = sa[...], sb[...]
        row = lax.broadcasted_iota(jnp.int32, (ROWS, LANE), 0)
        by = 1
        while by < ROWS:
            behind = row >= by
            b = jnp.where(behind, a * pltpu.roll(b, by, 0), 0.0) + b
            a = jnp.where(behind, pltpu.roll(a, by, 0), 1.0) * a
            by *= 2
        sa[...] = a
        sb[...] = b
        carry_out[0:1, :] = a[ROWS - 1 :, :]
        carry_out[1:2, :] = b[ROWS - 1 :, :]

        def tell(at, c):
            where = peer(at, c)
            launch(carry_out, carry_in.at[ep], k_send.at[CORES * at + c], k_recv.at[ep], (where, tp))

        tell(0, 1 - core)
        for at in range(1, RING):
            for c in range(CORES):
                tell(at, c)
        carry_in[ep] = carry_out[...]

    def mix_d():
        for at in range(RING):
            for c in range(CORES):
                if at == 0:
                    if c == 0:
                        who = peer(0, 1 - core)
                        arrived(who, k_recv, carry_in.at[who])
                else:
                    who = peer(at, c)
                    arrived(who, k_recv, carry_in.at[who])
        state = jnp.zeros((1, LANE), F32)
        for e in range(EP):
            pair = carry_in[e]
            state = jnp.where(e < ep, pair[0:1] * state + pair[1:2], state)
        lru = sb[...] + sa[...] * state
        mixer_out[...] = (lru * jax.nn.gelu(ybr[...].astype(F32), approximate=True)).astype(BF16)

    for what, k in ORDER:
        if what == "up":
            run_up(k)
        elif what == "down":
            run_down(k)
        elif what[:3] == "mix":
            {"A": mix_a, "B": mix_b, "C": mix_c, "D": mix_d}[what[3]]()
        else:
            gather(what[0], int(what[1]), k)

    arrived(1 - core, r_recv, ret.at[1 - core])
    for p in range(CORES, EP):
        arrived(p, r_recv, ret.at[p])
    back = ret[...].reshape(SLOTS, LANE)
    w = weight[...]
    total = w[:, 0:1] + w[:, 1:2]
    out = w[:, 0:1] / total * jnp.dot(c0[...], back, preferred_element_type=F32)
    out = out + w[:, 1:2] / total * jnp.dot(c1[...], back, preferred_element_type=F32)
    moe_out[...] = out.astype(BF16)
    for copy in pending:
        copy.wait_send()


def local(
    mix_in, mix_gain, w_in_x, w_in_y, conv_taps, recur_gate_w, input_gate_w, decay_logit, decay_shift,
    moe_in, moe_gain, routes, route_weight, expert_gate, expert_up, expert_down,
):
    anywhere = pl.BlockSpec(memory_space=pl.ANY)
    vmem = pl.BlockSpec(memory_space=pltpu.VMEM)
    dma = pltpu.SemaphoreType.DMA
    out = jax.ShapeDtypeStruct((ROWS, LANE), BF16)
    v = pltpu.VMEM
    return pl.pallas_call(
        kernel,
        out_shape=(out, out),
        in_specs=[anywhere] * 8 + [vmem] * 8,
        out_specs=(vmem, vmem),
        scratch_shapes=[
            v((ROWS, D), BF16), v((ROWS, D), BF16), v((D, 2 * LANE), BF16), v((ROWS, LANE), F32),
            v((D, 2 * LANE), BF16), v((D, LANE), BF16),
            v((ROWS, SLOTS), BF16), v((ROWS, SLOTS), BF16), v((EP, CAP, LANE), BF16),
            v((SIDE, SIDE, SLOTS, LANE), BF16), v((SIDE, SIDE, SLOTS, LANE), BF16),
            v((EP, CAP, LANE), BF16), v((EP, CAP, LANE), BF16),
            v((ROWS, LANE), BF16), v((ROWS + 8, LANE), F32), v((ROWS, LANE), BF16),
            v((16, LANE), BF16), v((16, LANE), BF16), v((ROWS, LANE), F32), v((ROWS, LANE), F32),
            v((2, LANE), F32), v((EP, 2, LANE), F32),
            dma((8,)), dma((2 * CHUNKS * 16,)), dma((2 * CHUNKS * 16,)), dma((EP,)), dma((EP,)),
            dma((EP,)), dma((EP,)), dma((EP,)), dma((EP,)), dma((2,)),
        ],
        compiler_params=pltpu.CompilerParams(
            collective_id=0, has_side_effects=True, vmem_limit_bytes=48 * 1024 * 1024
        ),
        name="mixer_and_experts",
    )(
        mix_in, moe_in, w_in_x, w_in_y, decay_shift, expert_gate, expert_up, expert_down,
        mix_gain.reshape(1, D), conv_taps, recur_gate_w, input_gate_w, decay_logit.reshape(1, LANE),
        moe_gain.reshape(1, D), routes, route_weight,
    )


def solution(mesh):
    placed = (
        P("ep", None),
        P(),
        P(None, "tp"),
        P(None, "tp"),
        P(None, "tp"),
        P("tp", None, None),
        P("tp", None, None),
        P("tp"),
        P("ep", "tp"),
        P("ep", None),
        P(),
        P("ep", None),
        P("ep", None),
        P("ep", None, "tp"),
        P("ep", None, "tp"),
        P("ep", None, "tp"),
    )
    return jax.shard_map(
        local, mesh=mesh, in_specs=placed, out_specs=(P("ep", "tp"), P("ep", "tp")), check_vma=False
    )
```

time: 252 us -> 105 us (0.42)
  waiting for transfers between devices: 134 us -> 0 us
  Pallas kernels: 0 us -> 93.1 us
  blocking collectives: 38.9 us -> 0 us
  starting transfers between devices: 31.1 us -> 0 us
  between operations: 15.2 us -> 0.71 us
  matrix products: 11.7 us -> 0 us
  other arithmetic: 5.83 us -> 0 us
  local copies, waits for them, and re-layouts: 14.7 us -> 11 us
    all_gather x2 -> x0, waiting for transfers between devices: 101 us -> none  [the longest x1 59.1 us: local(): piece = lax.all_gather(incoming, 'tp', axis=2, tiled=True)]
    pallas_call x0 -> x1, Pallas kernels: none -> 93.1 us  [local(): pl.pallas_call(kernel, out_shape=(out, out), in_specs=[anywhere] * 8 + [v...]
    all_to_all x1 -> x0, blocking collectives: 38.9 us -> none  [local(): lax.all_to_all(own_columns, 'ep', split_axis=0, concat_axis=0, tiled=True)]
    all_to_all x2 -> x0, waiting for transfers between devices: 32.8 us -> none  [the longest x1 20.9 us: local(): lax.all_to_all(results, 'ep', split_axis=0, concat_axis=0, tiled=True)]
    all_to_all x2 -> x0, starting transfers between devices: 28.8 us -> none  [the longest x1 14.4 us: copy_for_each(): lax.all_to_all(jnp.broadcast_to(value[None], (count, *value.shape)), axis...]
    dot_general x7 -> x0, matrix products: 11.7 us -> none  [the longest x1 4.15 us: local(): jnp.dot(lax.all_gather(hidden, 'tp', axis=1, tiled=True), down_rows, pref...]
    unnamed x33 -> x36, local copies, waits for them, and re-layouts: 1.01 us -> 11 us
    gather x2 -> x0, local copies, waits for them, and re-layouts: 7.31 us -> none  [the longest x1 5.97 us: local(): padded_rows[slot_owner].reshape(expert_count, capacity, feature_count)]
  transfers between devices with their start and end apart: 5 -> 0, of which waited for: 4 -> 0; matrix products, arithmetic and copies ran while one was open for 4% -> 0% of each run, Pallas kernels for 0% -> 0%
where the time goes in v1:
time: 105 us
  Pallas kernels  93.1 us (89%)
  local copies, waits for them, and re-layouts  11 us (10%)
    pallas_call x1, Pallas kernels, local(): pl.pallas_call(kernel, out_shape=(out, out), in_specs=[anywhere] * 8 + [v...  93.1 us
    unnamed x36, local copies, waits for them, and re-layouts  11 us

profile of v1, /device:TPU:1, one launch (start us, length us, event | category | flops | bytes accessed | tf_op | source)
XLA Modules:
  0.0 104.9 jit_solution(5763819290692063203)
XLA Ops:
  0.6 0.0 copy-start.14
  0.6 0.7 copy-done.14
  1.3 0.0 copy-start.15
  1.3 0.0 copy-start.7
  1.3 0.1 copy.18.routes
  1.5 0.5 copy-done.15
  2.0 0.0 copy-start.8
  2.0 0.0 copy-start.9
  2.0 0.0 copy-start.10
  2.0 0.0 copy-start.11
  2.0 0.0 copy-start.12
  2.0 0.0 copy-start.13
  2.0 0.1 copy.19.weight
  2.2 0.1 copy-done.7
  2.2 0.5 copy-done.8
  2.8 0.0 copy-done.9
  2.8 0.0 copy-done.10
  2.8 0.0 copy-done.11
  2.8 0.0 copy-done.12
  2.8 0.0 copy-done.13
  2.8 0.0 copy-start
  2.8 1.2 %copy-done = bf16[256,2048]{1,0:T(8,128)(2,1)S(1)} copy-done((bf16[256,2048]{1,0:T(8,128)(2,1)S(1)}, bf16[256,2048]{1,0:T(8,128)(2,1)}, u32[]{:S(2)}) %copy-start) | copy-done | bytes 1048600
  4.0 0.0 copy-start.1
  4.0 1.2 %copy-done.1 = bf16[256,2048]{1,0:T(8,128)(2,1)S(1)} copy-done((bf16[256,2048]{1,0:T(8,128)(2,1)S(1)}, bf16[256,2048]{1,0:T(8,128)(2,1)}, u32[]{:S(2)}) %copy-start.1) | copy-done | bytes 1048600
  5.3 0.0 copy-start.2
  5.3 1.0 copy-done.2
  6.3 0.0 copy-start.3
  6.3 1.0 copy-done.3
  7.3 0.0 copy-start.4
  7.3 1.0 copy-done.4
  8.4 0.0 copy-start.5
  8.4 1.0 copy-done.5
  9.4 0.0 copy-start.6
  9.4 1.0 copy-done.6
  10.5 93.1 %mixer_and_experts.1 = (bf16[256,128]{1,0:T(8,128)(2,1)S(1)}, bf16[256,128]{1,0:T(8,128)(2,1)S(1)}) custom-call(bf16[256,2048]{1,0:T(8,128)(2,1)S(1)} %copy-done, bf16[256,2048]{1,0:T(8,128)(2,1)S(1)} %copy-done.1, bf16[2048,128]{1,0:T(8,128)(2,1)S(1)} %copy-done.2, bf16[2048,128]{1,0:T(8,128)(2,1)S(1)} %copy-done.3, f32[256,128]{1,0:T(8,128)S(1)} %copy-done.7, ...), custom_call_target="tpu_custom_call" | custom-call | tf_op jit(solution)/shard_map/mixer_and_experts/pallas_call | solution.py:333
  103.6 0.6 copy.22
  104.2 0.6 copy.23
Async XLA Ops:
  0.6 0.7 copy-start.14
  1.3 0.7 copy-start.15
  1.3 0.9 copy-start.7
  2.0 0.8 copy-start.8
  2.0 0.8 copy-start.9
  2.0 0.8 copy-start.10
  2.0 0.8 copy-start.11
  2.0 0.8 copy-start.12
  2.0 0.8 copy-start.13
  2.8 1.2 %copy-start = (bf16[256,2048]{1,0:T(8,128)(2,1)S(1)}, bf16[256,2048]{1,0:T(8,128)(2,1)}, u32[]{:S(2)}) copy-start(bf16[256,2048]{1,0:T(8,128)(2,1)} %mix_in.1) | copy-start | bytes 3145732
  4.0 1.2 %copy-start.1 = (bf16[256,2048]{1,0:T(8,128)(2,1)S(1)}, bf16[256,2048]{1,0:T(8,128)(2,1)}, u32[]{:S(2)}) copy-start(bf16[256,2048]{1,0:T(8,128)(2,1)} %moe_in.1) | copy-start | bytes 3145732
  5.3 1.0 copy-start.2
  6.3 1.0 copy-start.3
  7.3 1.0 copy-start.4
  8.4 1.0 copy-start.5
  9.4 1.0 copy-start.6

commit v2 on v1

--- a/solution.py
+++ b/solution.py
@@ -27,11 +27,11 @@
 HALF = CH // 2
 QUARTER = HALF // 2
 
-NEAR = [0] + [s * d if s * d > -RING // 2 else RING // 2 for d in range(1, RING // 2 + 1) for s in (1, -1)][: RING - 1]
+NEAR = [0, 1, -1, 2, 8, 7, -7, 6, -6, 5, -5, -4, 4, 3, -3, -2]
 PLACE = {off % RING: at for at, off in enumerate(NEAR)}
 
 ORDER = [
-    ("R1", 0), ("mixA", 0), ("R2", 0), ("R1", 1), ("R3", 0), ("R2", 1), ("R1", 2), ("mixB", 0),
+    ("R1", 0), ("mixA", 0), ("R2", 0), ("R3", 0), ("mixB", 0), ("R1", 1), ("R2", 1), ("R1", 2),
     ("R4", 0), ("R3", 1), ("R2", 2), ("R1", 3), ("mixC", 0), ("up", 0), ("H1", 0),
     ("R4", 1), ("R3", 2), ("R2", 3), ("H2", 0), ("up", 1), ("H1", 1),
     ("R4", 2), ("R3", 3), ("H3", 0), ("H2", 1), ("up", 2), ("H1", 2),
@@ -59,6 +59,7 @@
     mix_gain, conv_taps, recur_w, input_w, logit, moe_gain, routes, weight,
     mixer_out, moe_out,
     mix_v, moe_v, win_v, shift_v, gu_v, down_v,
+    mix_gain_v, conv_taps_v, recur_v, input_v, logit_v, moe_gain_v, routes_v, weight_v,
     c0, c1, sent, X, H, res, ret, ybr, xb, xcv, halo_out, halo_in, sa, sb, carry_out, carry_in,
     load_sem, ag_send, ag_recv, d_send, d_recv, r_send, r_recv, k_send, k_recv, h_sem,
 ):
@@ -76,13 +77,22 @@
     def peer(at, c):
         return wrap(z + NEAR[at], RING) * CORES + c
 
-    loads = []
-    for n, (src, dst) in enumerate([
-        (moe_in, moe_v), (mix_in, mix_v), (w_x, win_v.at[:, :LANE]), (w_y, win_v.at[:, LANE:]), (shift, shift_v),
-        (w_gate.at[0], gu_v.at[:, :LANE]), (w_up.at[0], gu_v.at[:, LANE:]), (w_down.at[0], down_v),
+    loads = {}
+    for n, (name, src, dst) in enumerate([
+        ("routes", routes, routes_v), ("moe_gain", moe_gain, moe_gain_v), ("moe", moe_in, moe_v),
+        ("mix_gain", mix_gain, mix_gain_v), ("mix", mix_in, mix_v),
+        ("w_x", w_x, win_v.at[:, :LANE]), ("w_y", w_y, win_v.at[:, LANE:]),
+        ("taps", conv_taps, conv_taps_v), ("recur", recur_w, recur_v), ("input", input_w, input_v),
+        ("logit", logit, logit_v), ("shift", shift, shift_v),
+        ("gate", w_gate.at[0], gu_v.at[:, :LANE]), ("up", w_up.at[0], gu_v.at[:, LANE:]), ("down", w_down.at[0], down_v),
+        ("weight", weight, weight_v),
     ]):
-        loads.append(pltpu.make_async_copy(src, dst, load_sem.at[n]))
-        loads[-1].start()
+        loads[name] = pltpu.make_async_copy(src, dst, load_sem.at[n])
+        loads[name].start()
+
+    def loaded(*names):
+        for name in names:
+            loads[name].wait()
 
     barrier = pltpu.get_barrier_semaphore()
 
@@ -114,8 +124,14 @@
             return (v * scale * gain[:, lanes]).astype(BF16)
         return (v * scale * gain[...]).astype(BF16)
 
+    def columns(ref):
+        flat = ref[...].astype(F32)
+        return jnp.transpose(jnp.concatenate([flat] * 4, axis=0))
+
     lane_e = lax.broadcasted_iota(jnp.int32, (ROWS, LANE), 1)
-    onehot = [jnp.where(routes[:, k : k + 1] == lane_e, 1.0, 0.0).astype(BF16) for k in range(2)]
+    loaded("routes")
+    chosen = columns(routes_v).astype(jnp.int32)
+    onehot = [jnp.where(chosen[:, k : k + 1] == lane_e, 1.0, 0.0).astype(BF16) for k in range(2)]
     before = jnp.where(
         lax.broadcasted_iota(jnp.int32, (ROWS, ROWS), 1) < lax.broadcasted_iota(jnp.int32, (ROWS, ROWS), 0), 1.0, 0.0
     ).astype(BF16)
@@ -123,21 +139,24 @@
     rank[1] = rank[1] + jnp.sum(onehot[0].astype(F32), axis=0, keepdims=True)
     lane_1 = lax.broadcasted_iota(jnp.int32, (1, LANE), 1)
     off = (lane_1 // CORES - z + 2 * RING) % RING
-    at = jnp.where(off == 0, 0, jnp.where(off <= RING // 2, 2 * off - 1, 2 * (RING - off)))
+    at = jnp.zeros((1, LANE), jnp.int32)
+    for n in range(1, RING):
+        at = jnp.where(off == NEAR[n] % RING, n, at)
     base = (CAP * (CORES * at + lane_1 % CORES)).astype(F32)
     slot_lane = lax.broadcasted_iota(jnp.int32, (ROWS, SLOTS), 1)
     for ref, hot, r in zip((c0, c1), onehot, rank):
         slot = jnp.sum(hot.astype(F32) * (r + base), axis=1, keepdims=True).astype(jnp.int32)
         ref[...] = jnp.where(slot_lane == slot, 1.0, 0.0).astype(BF16)
 
-    loads[0].wait()
+    loaded("moe", "moe_gain")
     own_lanes = pl.ds(pl.multiple_of(tp * LANE, LANE), LANE)
-    own_rows = normed(moe_v, moe_gain, own_lanes)
+    own_rows = normed(moe_v, moe_gain_v, own_lanes)
     sent[...] = lax.dot_general(
         c0[...] + c1[...], own_rows, (((0,), (0,)), ((), ())), preferred_element_type=F32
     ).astype(BF16).reshape(EP, CAP, LANE)
 
-    pl.semaphore_wait(barrier, len(plane) + EP - 1)
+    with jax.named_scope("barrier"):
+        pl.semaphore_wait(barrier, len(plane) + EP - 1)
 
     def block(buf, p):
         return buf.at[y, x, pl.ds(pl.multiple_of(p * CAP, CAP), CAP)]
@@ -203,8 +222,7 @@
         for n in range(4):
             ways["R", 4, k, n].wait_recv()
         if k == 0:
-            loads[5].wait()
-            loads[6].wait()
+            loaded("gate", "up")
         both = jnp.dot(all_blocks(X, k), gu_v[...], preferred_element_type=F32)
         g, u = both[:, :LANE], both[:, LANE:]
         H[y, x, pl.ds(k * CH, CH), :] = (g * jax.nn.sigmoid(g) * u).astype(BF16)
@@ -213,7 +231,7 @@
         for n in range(4):
             ways["H", 4, k, n].wait_recv()
         if k == 0:
-            loads[7].wait()
+            loaded("down")
         out = jnp.dot(all_blocks(H, k), down_v[...], preferred_element_type=F32).astype(BF16)
         first = k * CH // CAP
         res[pl.ds(first, CH // CAP)] = out.reshape(CH // CAP, CAP, LANE)
@@ -232,10 +250,8 @@
                 give(at, c, peer(at, c))
 
     def mix_a():
-        loads[1].wait()
-        loads[2].wait()
-        loads[3].wait()
-        rows = normed(mix_v, mix_gain, None)
+        loaded("mix", "mix_gain", "w_x", "w_y")
+        rows = normed(mix_v, mix_gain_v, None)
         both = jnp.dot(rows, win_v[...], preferred_element_type=F32).astype(BF16)
         ybr[...] = both[:, LANE:]
         xb[pl.ds(8, ROWS), :] = both[:, :LANE].astype(F32)
@@ -244,16 +260,16 @@
 
     def mix_b():
         ways["halo"].wait_recv()
+        loaded("taps", "recur", "input", "logit", "shift")
         xb[pl.ds(0, 8), :] = jnp.where(ep > 0, halo_in[...].astype(F32)[8:], 0.0)
         conv = jnp.zeros((ROWS, LANE), F32)
         for k in range(4):
-            conv = conv + conv_taps[k : k + 1, :] * xb[pl.ds(5 + k, ROWS), :]
+            conv = conv + conv_taps_v[k : k + 1, :] * xb[pl.ds(5 + k, ROWS), :]
         x_conv = conv.astype(BF16)
         xcv[...] = x_conv
-        gate_a = jnp.dot(x_conv, recur_w[0], preferred_element_type=F32)
-        gate_x = jnp.dot(x_conv, input_w[0], preferred_element_type=F32)
-        loads[4].wait()
-        log_decay = -lru_scale * jax.nn.sigmoid(gate_a) * softplus(-logit[...]) + shift_v[...]
+        gate_a = jnp.dot(x_conv, recur_v[0], preferred_element_type=F32)
+        gate_x = jnp.dot(x_conv, input_v[0], preferred_element_type=F32)
+        log_decay = -lru_scale * jax.nn.sigmoid(gate_a) * softplus(-logit_v[...]) + shift_v[...]
         sa[...] = jnp.exp(log_decay)
         sb[...] = jnp.sqrt(one_minus_exp(2.0 * log_decay)) * jax.nn.sigmoid(gate_x) * x_conv.astype(F32)
 
@@ -299,33 +315,37 @@
         mixer_out[...] = (lru * jax.nn.gelu(ybr[...].astype(F32), approximate=True)).astype(BF16)
 
     for what, k in ORDER:
-        if what == "up":
-            run_up(k)
-        elif what == "down":
-            run_down(k)
-        elif what[:3] == "mix":
-            {"A": mix_a, "B": mix_b, "C": mix_c, "D": mix_d}[what[3]]()
-        else:
-            gather(what[0], int(what[1]), k)
-
-    arrived(1 - core, r_recv, ret.at[1 - core])
-    for p in range(CORES, EP):
-        arrived(p, r_recv, ret.at[p])
+        with jax.named_scope(f"{what}_{k}"):
+            if what == "up":
+                run_up(k)
+            elif what == "down":
+                run_down(k)
+            elif what[:3] == "mix":
+                {"A": mix_a, "B": mix_b, "C": mix_c, "D": mix_d}[what[3]]()
+            else:
+                gather(what[0], int(what[1]), k)
+
+    with jax.named_scope("back"):
+        arrived(1 - core, r_recv, ret.at[1 - core])
+        for p in range(CORES, EP):
+            arrived(p, r_recv, ret.at[p])
     back = ret[...].reshape(SLOTS, LANE)
-    w = weight[...]
+    loaded("weight")
+    w = columns(weight_v)
     total = w[:, 0:1] + w[:, 1:2]
     out = w[:, 0:1] / total * jnp.dot(c0[...], back, preferred_element_type=F32)
     out = out + w[:, 1:2] / total * jnp.dot(c1[...], back, preferred_element_type=F32)
     moe_out[...] = out.astype(BF16)
-    for copy in pending:
-        copy.wait_send()
+    with jax.named_scope("sends"):
+        for copy in pending:
+            copy.wait_send()
 
 
 def local(
     mix_in, mix_gain, w_in_x, w_in_y, conv_taps, recur_gate_w, input_gate_w, decay_logit, decay_shift,
     moe_in, moe_gain, routes, route_weight, expert_gate, expert_up, expert_down,
 ):
-    anywhere = pl.BlockSpec(memory_space=pl.ANY)
+    hbm = pl.BlockSpec(memory_space=pltpu.HBM)
     vmem = pl.BlockSpec(memory_space=pltpu.VMEM)
     dma = pltpu.SemaphoreType.DMA
     out = jax.ShapeDtypeStruct((ROWS, LANE), BF16)
@@ -333,28 +353,30 @@
     return pl.pallas_call(
         kernel,
         out_shape=(out, out),
-        in_specs=[anywhere] * 8 + [vmem] * 8,
+        in_specs=[hbm] * 16,
         out_specs=(vmem, vmem),
         scratch_shapes=[
             v((ROWS, D), BF16), v((ROWS, D), BF16), v((D, 2 * LANE), BF16), v((ROWS, LANE), F32),
             v((D, 2 * LANE), BF16), v((D, LANE), BF16),
+            v((1, D), F32), v((4, LANE), F32), v((1, LANE, LANE), BF16), v((1, LANE, LANE), BF16), v((1, LANE), F32),
+            v((1, D), F32), v((2, ROWS), jnp.int32), v((2, ROWS), F32),
             v((ROWS, SLOTS), BF16), v((ROWS, SLOTS), BF16), v((EP, CAP, LANE), BF16),
             v((SIDE, SIDE, SLOTS, LANE), BF16), v((SIDE, SIDE, SLOTS, LANE), BF16),
             v((EP, CAP, LANE), BF16), v((EP, CAP, LANE), BF16),
             v((ROWS, LANE), BF16), v((ROWS + 8, LANE), F32), v((ROWS, LANE), BF16),
             v((16, LANE), BF16), v((16, LANE), BF16), v((ROWS, LANE), F32), v((ROWS, LANE), F32),
             v((2, LANE), F32), v((EP, 2, LANE), F32),
-            dma((8,)), dma((2 * CHUNKS * 16,)), dma((2 * CHUNKS * 16,)), dma((EP,)), dma((EP,)),
+            dma((16,)), dma((2 * CHUNKS * 16,)), dma((2 * CHUNKS * 16,)), dma((EP,)), dma((EP,)),
             dma((EP,)), dma((EP,)), dma((EP,)), dma((EP,)), dma((2,)),
         ],
         compiler_params=pltpu.CompilerParams(
-            collective_id=0, has_side_effects=True, vmem_limit_bytes=48 * 1024 * 1024
+            collective_id=0, has_side_effects=True, vmem_limit_bytes=67043328
         ),
         name="mixer_and_experts",
     )(
         mix_in, moe_in, w_in_x, w_in_y, decay_shift, expert_gate, expert_up, expert_down,
         mix_gain.reshape(1, D), conv_taps, recur_gate_w, input_gate_w, decay_logit.reshape(1, LANE),
-        moe_gain.reshape(1, D), routes, route_weight,
+        moe_gain.reshape(1, D), routes.T, route_weight.T,
     )
 
 

time: 105 us -> 105 us (level)
  Pallas kernels: 93.1 us -> 102 us
  local copies, waits for them, and re-layouts: 11 us -> 2.14 us
    pallas_call x1, Pallas kernels: 93.1 us -> 102 us  [local(): pl.pallas_call(kernel, out_shape=(out, out), in_specs=[hbm] * 16, out_spe...]
    unnamed x36 -> x4, local copies, waits for them, and re-layouts: 11 us -> 2.14 us
where the time goes in v2:
time: 105 us
  Pallas kernels  102 us (97%)
  local copies, waits for them, and re-layouts  2.14 us (2%)
    pallas_call x1, Pallas kernels, local(): pl.pallas_call(kernel, out_shape=(out, out), in_specs=[hbm] * 16, out_spe...  102 us
    unnamed x4, local copies, waits for them, and re-layouts  2.14 us

profile of v2, /device:TPU:1, one launch (start us, length us, event | category | flops | bytes accessed | tf_op | source)
XLA Modules:
  0.0 104.9 jit_solution(1031137642409088460)
XLA Ops:
  0.6 102.1 %mixer_and_experts.1 = (bf16[256,128]{1,0:T(8,128)(2,1)}, bf16[256,128]{1,0:T(8,128)(2,1)}) custom-call(bf16[256,2048]{1,0:T(8,128)(2,1)} %mix_in.1, bf16[256,2048]{1,0:T(8,128)(2,1)} %moe_in.1, bf16[2048,128]{1,0:T(8,128)(2,1)} %w_x.1, bf16[2048,128]{1,0:T(8,128)(2,1)} %w_y.1, f32[256,128]{1,0:T(8,128)} %shift.1, bf16[1,2048,128]{2,1,0:T(8,128)(2,1)} %w_gate.1, ...), custom_call_target="tpu_custom_call" | custom-call | tf_op jit(solution)/shard_map/mixer_and_experts/pallas_call | solution.py:353
  102.8 0.0 copy-start
  102.8 1.5 %copy.20 = bf16[256,128]{1,0:T(8,128)(2,1)} copy(bf16[256,128]{1,0:T(8,128)(2,1)} %get-tuple-element.4) | data formatting | bytes 131072
  104.3 0.0 copy-done
  104.3 0.6 copy.21
Async XLA Ops:
  102.8 1.5 %copy-start = (bf16[256,128]{1,0:T(8,128)(2,1)S(1)}, bf16[256,128]{1,0:T(8,128)(2,1)}, u32[]{:S(2)}) copy-start(bf16[256,128]{1,0:T(8,128)(2,1)} %get-tuple-element.5) | copy-start | bytes 196612

commit v3 on v2

--- a/solution.py
+++ b/solution.py
@@ -24,21 +24,22 @@
 SLOTS = EP * CAP
 CHUNKS = 4
 CH = SLOTS // CHUNKS
-HALF = CH // 2
-QUARTER = HALF // 2
-
-NEAR = [0, 1, -1, 2, 8, 7, -7, 6, -6, 5, -5, -4, 4, 3, -3, -2]
+QROWS = CH // SIDE
+PIECES = 8
+WROWS = D // PIECES
+
+XROWS = [128, 128, 128, 128]
+
+NEAR = [0, 1, -1, 2, -7, 7, 6, 8, 5, -6, -4, -5, 4, -3, 3, -2]
 PLACE = {off % RING: at for at, off in enumerate(NEAR)}
 
 ORDER = [
-    ("R1", 0), ("mixA", 0), ("R2", 0), ("R3", 0), ("mixB", 0), ("R1", 1), ("R2", 1), ("R1", 2),
-    ("R4", 0), ("R3", 1), ("R2", 2), ("R1", 3), ("mixC", 0), ("up", 0), ("H1", 0),
-    ("R4", 1), ("R3", 2), ("R2", 3), ("H2", 0), ("up", 1), ("H1", 1),
-    ("R4", 2), ("R3", 3), ("H3", 0), ("H2", 1), ("up", 2), ("H1", 2),
-    ("R4", 3), ("H4", 0), ("H3", 1), ("H2", 2), ("up", 3), ("H1", 3), ("mixD", 0),
-    ("down", 0), ("H4", 1), ("H3", 2), ("H2", 3),
-    ("down", 1), ("H4", 2), ("H3", 3), ("down", 2), ("H4", 3), ("down", 3),
+    "MA0", "Y10", "X10", "W16", "Y20", "X20", "Y30", "W21", "X30", "MB0", "MC0", "Y11", "X11", "Y40", "X40", "Y12",
+    "X12", "Y21", "X21", "Y22", "Y31", "X22", "Y13", "X13", "X31", "Y32", "Y23", "Y41", "X32", "X23", "UP0", "X41",
+    "MD0", "Y33", "Y42", "W17", "W20", "X42", "X33", "B10", "UP1", "Y43", "W23", "B20", "UP2", "X43", "W22", "B11",
+    "B12", "UP3", "B21", "DN0", "B13", "B22", "DN1", "B23", "DN2", "DN3",
 ]
+EARLY = 6
 
 
 def softplus(v):
@@ -58,10 +59,11 @@
     mix_in, moe_in, w_x, w_y, shift, w_gate, w_up, w_down,
     mix_gain, conv_taps, recur_w, input_w, logit, moe_gain, routes, weight,
     mixer_out, moe_out,
-    mix_v, moe_v, win_v, shift_v, gu_v, down_v,
+    mix_v, moe_v, win_v, shift_v, gu_v, wd,
     mix_gain_v, conv_taps_v, recur_v, input_v, logit_v, moe_gain_v, routes_v, weight_v,
-    c0, c1, sent, X, H, res, ret, ybr, xb, xcv, halo_out, halo_in, sa, sb, carry_out, carry_in,
-    load_sem, ag_send, ag_recv, d_send, d_recv, r_send, r_recv, k_send, k_recv, h_sem,
+    c0, c1, sent, X, hown, H, res, ret, ybr, xb, xcv, halo_out, halo_in, sa, sb, carry_out, carry_in,
+    load_sem, x_send, x_recv, b_send, b_recv, a_send, a_recv, w_send, w_recv,
+    d_send, d_recv, r_send, r_recv, k_send, k_recv, h_sem,
 ):
     ep, tp = lax.axis_index("ep"), lax.axis_index("tp")
     z, core = ep // CORES, lax.rem(ep, CORES)
@@ -72,19 +74,33 @@
 
     east, west = wrap(x + 1, SIDE), wrap(x - 1, SIDE)
     north, south = wrap(y + 1, SIDE), wrap(y - 1, SIDE)
+    across = wrap(x + 2, SIDE)
     plane = [(ep, y * SIDE + east), (ep, y * SIDE + west), (ep, north * SIDE + x), (ep, south * SIDE + x)]
+    row = [plane[0], plane[1], (ep, y * SIDE + across)]
+
+    def by_x(values, of):
+        got = values[0]
+        for n in range(1, SIDE):
+            got = jnp.where(of == n, values[n], got)
+        return got
+
+    def offset(k, of):
+        return by_x(NEAR[SIDE * k : SIDE * (k + 1)], of)
+
+    def lanes(n):
+        return pl.ds(pl.multiple_of(n * LANE, LANE), LANE)
 
     def peer(at, c):
         return wrap(z + NEAR[at], RING) * CORES + c
 
     loads = {}
     for n, (name, src, dst) in enumerate([
-        ("routes", routes, routes_v), ("moe_gain", moe_gain, moe_gain_v), ("moe", moe_in, moe_v),
+        ("routes", routes, routes_v), ("down", w_down.at[0], wd.at[:, lanes(x)]), ("moe_gain", moe_gain, moe_gain_v), ("moe", moe_in, moe_v),
         ("mix_gain", mix_gain, mix_gain_v), ("mix", mix_in, mix_v),
         ("w_x", w_x, win_v.at[:, :LANE]), ("w_y", w_y, win_v.at[:, LANE:]),
         ("taps", conv_taps, conv_taps_v), ("recur", recur_w, recur_v), ("input", input_w, input_v),
         ("logit", logit, logit_v), ("shift", shift, shift_v),
-        ("gate", w_gate.at[0], gu_v.at[:, :LANE]), ("up", w_up.at[0], gu_v.at[:, LANE:]), ("down", w_down.at[0], down_v),
+        ("gate", w_gate.at[0], gu_v.at[:, :LANE]), ("up", w_up.at[0], gu_v.at[:, LANE:]),
         ("weight", weight, weight_v),
     ]):
         loads[name] = pltpu.make_async_copy(src, dst, load_sem.at[n])
@@ -99,12 +115,19 @@
     def greet(where):
         pl.semaphore_signal(barrier, inc=1, device_id=where, device_id_type=MESH)
 
-    for where in plane:
+    for where in plane + row[2:]:
         greet(where)
     greet((peer(0, 1 - core), tp))
     for at in range(1, RING):
         for c in range(CORES):
             greet((peer(at, c), tp))
+    for k in range(CHUNKS):
+        for by in range(1, SIDE):
+            other = wrap(x + by, SIDE)
+            for c in range(CORES):
+                greet((wrap(z + offset(k, x), RING) * CORES + c, y * SIDE + other))
+                greet((wrap(z - offset(k, other), RING) * CORES + c, y * SIDE + other))
+    greeted = len(plane) + 1 + EP - 1 + 2 * CHUNKS * (SIDE - 1) * CORES
 
     pending = []
 
@@ -148,106 +171,176 @@
         slot = jnp.sum(hot.astype(F32) * (r + base), axis=1, keepdims=True).astype(jnp.int32)
         ref[...] = jnp.where(slot_lane == slot, 1.0, 0.0).astype(BF16)
 
+    with jax.named_scope("barrier"):
+        pl.semaphore_wait(barrier, greeted)
+    loaded("down")
+    ways = {}
+
+    def weights(step, q):
+        if step == 1:
+            views = [(wd.at[pl.ds(q * WROWS, WROWS), lanes(x)], q)] * 2
+        else:
+            ways["W", 1, q, 0].wait_recv()
+            ways["W", 1, q + PIECES // 2, 1].wait_recv()
+            views = [
+                (wd.at[pl.ds(q * WROWS, WROWS), lanes(west)], PIECES + q),
+                (wd.at[pl.ds((q + PIECES // 2) * WROWS, WROWS), lanes(east)], PIECES + q),
+            ]
+        for n, (view, slot) in enumerate(views):
+            ways["W", step, q, n] = launch(view, view, w_send.at[2 * slot + n], w_recv.at[2 * slot + n], row[n])
+
+    for q in range(EARLY):
+        weights(1, q)
+
     loaded("moe", "moe_gain")
-    own_lanes = pl.ds(pl.multiple_of(tp * LANE, LANE), LANE)
-    own_rows = normed(moe_v, moe_gain_v, own_lanes)
+    own_rows = normed(moe_v, moe_gain_v, lanes(tp))
     sent[...] = lax.dot_general(
         c0[...] + c1[...], own_rows, (((0,), (0,)), ((), ())), preferred_element_type=F32
     ).astype(BF16).reshape(EP, CAP, LANE)
 
-    with jax.named_scope("barrier"):
-        pl.semaphore_wait(barrier, len(plane) + EP - 1)
-
     def block(buf, p):
         return buf.at[y, x, pl.ds(pl.multiple_of(p * CAP, CAP), CAP)]
 
-    def dispatch(at, c, where):
-        place = PLACE[-NEAR[at] % RING] * CORES + core
-        launch(sent.at[CORES * at + c], block(X, place), d_send.at[CORES * at + c], d_recv.at[place], (where, tp))
-
-    dispatch(0, 1 - core, peer(0, 1 - core))
+    def dispatch(at, c):
+        local = CORES * PLACE[-NEAR[at] % RING] + c
+        place = CORES * at + core
+        where = wrap(z - NEAR[at], RING) * CORES + c
+        launch(sent.at[local], block(X, place), d_send.at[local], d_recv.at[place], (where, tp))
+
+    dispatch(0, 1 - core)
     for at in range(1, RING):
         for c in range(CORES):
-            dispatch(at, c, peer(at, c))
+            dispatch(at, c)
     own = pl.ds(pl.multiple_of(core * CAP, CAP), CAP)
     X[y, x, own, :] = sent[core]
 
-    def arrived(p, sem, buf_block):
+    def arrived(p, sem, ref):
         pltpu.make_async_remote_copy(
-            src_ref=buf_block, dst_ref=buf_block, send_sem=sem.at[p], recv_sem=sem.at[p],
+            src_ref=ref, dst_ref=ref, send_sem=sem.at[p], recv_sem=sem.at[p],
             device_id=(ep, tp), device_id_type=MESH,
         ).wait_recv()
 
     def await_dispatch(k):
+        if ("in", k) in ways:
+            return
+        ways["in", k] = None
         for p in range(k * CH // CAP, (k + 1) * CH // CAP):
-            if p < CORES:
-                if p == 0:
-                    arrived(1 - core, d_recv, block(X, 1 - core))
-            else:
+            if p >= CORES:
                 arrived(p, d_recv, block(X, p))
-
-    bufs = {"R": X, "H": H}
-    ways = {}
-
-    def gather(kind, step, k):
-        buf = bufs[kind]
-        lo = k * CH
-        xs, ys = pl.ds(lo, HALF), pl.ds(lo + HALF, HALF)
-        xa, xz = pl.ds(lo, QUARTER), pl.ds(lo + QUARTER, QUARTER)
-        ya, yz = pl.ds(lo + HALF, QUARTER), pl.ds(lo + HALF + QUARTER, QUARTER)
+            elif p == 0:
+                arrived(1 - core, d_recv, block(X, 1 - core))
+
+    def gather(part, step, k):
+        lo, size = k * CH, XROWS[k]
+        if part == "Y":
+            lo, size = lo + size, CH - size
+        full, first, second = pl.ds(lo, size), pl.ds(lo, size // 2), pl.ds(lo + size // 2, size // 2)
+        along_x = (part == "X") == (step < 3)
         if step == 1:
-            if kind == "R":
-                await_dispatch(k)
-            views = [buf.at[y, x, xs], buf.at[y, x, xs], buf.at[y, x, ys], buf.at[y, x, ys]]
+            await_dispatch(k)
+            views = [X.at[y, x, full]] * 2
+        elif step == 2 and along_x:
+            views = [X.at[y, west, first], X.at[y, east, second]]
         elif step == 2:
-            views = [buf.at[y, west, xa], buf.at[y, east, xz], buf.at[south, x, ya], buf.at[north, x, yz]]
+            views = [X.at[south, x, first], X.at[north, x, second]]
+        elif step == 3 and along_x:
+            views = [X.at[:, x, full]] * 2
         elif step == 3:
-            views = [buf.at[:, x, ys], buf.at[:, x, ys], buf.at[y, :, xs], buf.at[y, :, xs]]
+            views = [X.at[y, :, full]] * 2
+        elif along_x:
+            views = [X.at[:, west, first], X.at[:, east, second]]
         else:
-            views = [buf.at[:, west, ya], buf.at[:, east, yz], buf.at[south, :, xa], buf.at[north, :, xz]]
+            views = [X.at[south, :, first], X.at[north, :, second]]
         if step == 3:
-            for n in range(4):
-                ways[kind, 2, k, n].wait_recv()
-        for n in range(4):
+            for n in range(2):
+                ways[part, 2, k, n].wait_recv()
+        for n in range(2):
             if step == 2 or step == 4:
-                ways[kind, step - 1, k, n].wait_recv()
-            slot = (("RH".index(kind) * CHUNKS + k) * 4 + step - 1) * 4 + n
-            ways[kind, step, k, n] = launch(views[n], views[n], ag_send.at[slot], ag_recv.at[slot], plane[n])
-
-    def all_blocks(buf, k):
-        rows = pl.ds(k * CH, CH)
+                ways[part, step - 1, k, n].wait_recv()
+            slot = ((("XY".index(part) * CHUNKS) + k) * 4 + step - 1) * 2 + n
+            ways[part, step, k, n] = launch(
+                views[n], views[n], x_send.at[slot], x_recv.at[slot], plane[n if along_x else 2 + n]
+            )
+
+    def all_blocks(buf, rows):
         return jnp.concatenate([buf[a, b, rows, :] for a in range(SIDE) for b in range(SIDE)], axis=1)
 
+    def quarter(k, n):
+        return pl.ds(pl.multiple_of(k * CH + n * QROWS, QROWS), QROWS)
+
     def run_up(k):
-        for n in range(4):
-            ways["R", 4, k, n].wait_recv()
+        for part in "XY":
+            for n in range(2):
+                ways[part, 4, k, n].wait_recv()
         if k == 0:
             loaded("gate", "up")
-        both = jnp.dot(all_blocks(X, k), gu_v[...], preferred_element_type=F32)
+        both = jnp.dot(all_blocks(X, pl.ds(k * CH, CH)), gu_v[...], preferred_element_type=F32)
         g, u = both[:, :LANE], both[:, LANE:]
-        H[y, x, pl.ds(k * CH, CH), :] = (g * jax.nn.sigmoid(g) * u).astype(BF16)
+        hown[pl.ds(k * CH, CH), :] = (g * jax.nn.sigmoid(g) * u).astype(BF16)
+        mine = pl.ds(k * QROWS, QROWS)
+        for n, who in enumerate((east, west, across)):
+            slot = 3 * k + n
+            ways["A", k, n] = launch(hown.at[quarter(k, who)], H.at[y, x, mine], a_send.at[slot], a_recv.at[slot], row[n])
+        H[y, x, mine, :] = hown[quarter(k, x), :]
+
+    def spread(step, k):
+        slot = 4 * k + 2 * (step - 1)
+        lo = k * QROWS
+        if step == 1:
+            for n, who in enumerate((west, east, across)):
+                ways["A", k, n].wait_recv()
+            views = [H.at[y, :, pl.ds(lo, QROWS)]] * 2
+        else:
+            views = [H.at[south, :, pl.ds(lo, QROWS // 2)], H.at[north, :, pl.ds(lo + QROWS // 2, QROWS // 2)]]
+        for n in range(2):
+            if step == 2:
+                ways["B", 1, k, n].wait_recv()
+            ways["B", step, k, n] = launch(views[n], views[n], b_send.at[slot + n], b_recv.at[slot + n], plane[2 + n])
+
+    def give(k, c, by, act):
+        other = wrap(x + by, SIDE)
+        off = offset(k, x)
+        place = by_x([PLACE[-v % RING] for v in NEAR[SIDE * k : SIDE * (k + 1)]], x) * CORES + core
+        slot = (k * CORES + c) * SIDE + by
+        copy = pltpu.make_async_remote_copy(
+            src_ref=res.at[k * CORES + c, other], dst_ref=ret.at[place], send_sem=r_send.at[slot], recv_sem=r_recv.at[place],
+            device_id=(wrap(z + off, RING) * CORES + c, y * SIDE + other), device_id_type=MESH,
+        )
+        if k == 0 and by == 0:
+            stays = jnp.logical_and(x == 0, core == c)
+
+            @pl.when(jnp.logical_not(stays))
+            def _():
+                act(copy)
+
+            if act is starts:
+
+                @pl.when(stays)
+                def _():
+                    ret[core] = res[c, 0]
+
+        else:
+            act(copy)
+
+    def starts(copy):
+        copy.start()
 
     def run_down(k):
-        for n in range(4):
-            ways["H", 4, k, n].wait_recv()
+        for n in range(2):
+            ways["B", 2, k, n].wait_recv()
         if k == 0:
-            loaded("down")
-        out = jnp.dot(all_blocks(H, k), down_v[...], preferred_element_type=F32).astype(BF16)
-        first = k * CH // CAP
-        res[pl.ds(first, CH // CAP)] = out.reshape(CH // CAP, CAP, LANE)
-
-        def give(at, c, where):
-            place = PLACE[-NEAR[at] % RING] * CORES + core
-            launch(res.at[CORES * at + c], ret.at[place], r_send.at[CORES * at + c], r_recv.at[place], (where, tp))
-
-        for p in range(first, first + CH // CAP):
-            at, c = p // CORES, p % CORES
-            if at == 0:
-                if c == 0:
-                    give(0, 1 - core, peer(0, 1 - core))
-                    ret[core] = res[core]
-            else:
-                give(at, c, peer(at, c))
+            for q in range(PIECES // 2):
+                ways["W", 1, q, 1].wait_recv()
+                ways["W", 1, q + PIECES // 2, 0].wait_recv()
+                ways["W", 2, q, 0].wait_recv()
+                ways["W", 2, q, 1].wait_recv()
+        out = jnp.dot(all_blocks(H, pl.ds(k * QROWS, QROWS)), wd[...], preferred_element_type=F32).astype(BF16)
+        for n in range(SIDE):
+            for c in range(CORES):
+                res[k * CORES + c, n] = out[c * CAP : (c + 1) * CAP, n * LANE : (n + 1) * LANE]
+        for by in range(SIDE):
+            for c in range(CORES):
+                give(k, c, by, starts)
 
     def mix_a():
         loaded("mix", "mix_gain", "w_x", "w_y")
@@ -300,12 +393,8 @@
     def mix_d():
         for at in range(RING):
             for c in range(CORES):
-                if at == 0:
-                    if c == 0:
-                        who = peer(0, 1 - core)
-                        arrived(who, k_recv, carry_in.at[who])
-                else:
-                    who = peer(at, c)
+                if at > 0 or c == 0:
+                    who = peer(at, c) if at else peer(0, 1 - core)
                     arrived(who, k_recv, carry_in.at[who])
         state = jnp.zeros((1, LANE), F32)
         for e in range(EP):
@@ -314,14 +403,19 @@
         lru = sb[...] + sa[...] * state
         mixer_out[...] = (lru * jax.nn.gelu(ybr[...].astype(F32), approximate=True)).astype(BF16)
 
-    for what, k in ORDER:
+    for item in ORDER:
+        what, k = item[:-1], int(item[-1])
         with jax.named_scope(f"{what}_{k}"):
-            if what == "up":
+            if what == "UP":
                 run_up(k)
-            elif what == "down":
+            elif what == "DN":
                 run_down(k)
-            elif what[:3] == "mix":
-                {"A": mix_a, "B": mix_b, "C": mix_c, "D": mix_d}[what[3]]()
+            elif what[0] == "M":
+                {"A": mix_a, "B": mix_b, "C": mix_c, "D": mix_d}[what[1]]()
+            elif what[0] == "W":
+                weights(int(what[1]), k)
+            elif what[0] == "B":
+                spread(int(what[1]), k)
             else:
                 gather(what[0], int(what[1]), k)
 
@@ -329,6 +423,11 @@
         arrived(1 - core, r_recv, ret.at[1 - core])
         for p in range(CORES, EP):
             arrived(p, r_recv, ret.at[p])
+
+        @pl.when(x != 0)
+        def _():
+            arrived(core, r_recv, ret.at[core])
+
     back = ret[...].reshape(SLOTS, LANE)
     loaded("weight")
     w = columns(weight_v)
@@ -339,6 +438,10 @@
     with jax.named_scope("sends"):
         for copy in pending:
             copy.wait_send()
+        for k in range(CHUNKS):
+            for by in range(SIDE):
+                for c in range(CORES):
+                    give(k, c, by, lambda copy: copy.wait_send())
 
 
 def local(
@@ -357,16 +460,17 @@
         out_specs=(vmem, vmem),
         scratch_shapes=[
             v((ROWS, D), BF16), v((ROWS, D), BF16), v((D, 2 * LANE), BF16), v((ROWS, LANE), F32),
-            v((D, 2 * LANE), BF16), v((D, LANE), BF16),
+            v((D, 2 * LANE), BF16), v((D, SIDE * LANE), BF16),
             v((1, D), F32), v((4, LANE), F32), v((1, LANE, LANE), BF16), v((1, LANE, LANE), BF16), v((1, LANE), F32),
             v((1, D), F32), v((2, ROWS), jnp.int32), v((2, ROWS), F32),
             v((ROWS, SLOTS), BF16), v((ROWS, SLOTS), BF16), v((EP, CAP, LANE), BF16),
-            v((SIDE, SIDE, SLOTS, LANE), BF16), v((SIDE, SIDE, SLOTS, LANE), BF16),
-            v((EP, CAP, LANE), BF16), v((EP, CAP, LANE), BF16),
+            v((SIDE, SIDE, SLOTS, LANE), BF16), v((SLOTS, LANE), BF16), v((SIDE, SIDE, SLOTS // SIDE, LANE), BF16),
+            v((CHUNKS * CORES, SIDE, CAP, LANE), BF16), v((EP, CAP, LANE), BF16),
             v((ROWS, LANE), BF16), v((ROWS + 8, LANE), F32), v((ROWS, LANE), BF16),
             v((16, LANE), BF16), v((16, LANE), BF16), v((ROWS, LANE), F32), v((ROWS, LANE), F32),
             v((2, LANE), F32), v((EP, 2, LANE), F32),
-            dma((16,)), dma((2 * CHUNKS * 16,)), dma((2 * CHUNKS * 16,)), dma((EP,)), dma((EP,)),
+            dma((16,)), dma((CHUNKS * 16,)), dma((CHUNKS * 16,)), dma((CHUNKS * 4,)), dma((CHUNKS * 4,)),
+            dma((CHUNKS * 3,)), dma((CHUNKS * 3,)), dma((PIECES * 3,)), dma((PIECES * 3,)), dma((EP,)), dma((EP,)),
             dma((EP,)), dma((EP,)), dma((EP,)), dma((EP,)), dma((2,)),
         ],
         compiler_params=pltpu.CompilerParams(

time: 105 us -> 95.2 us (0.907)
  Pallas kernels: 102 us -> 92.2 us
    pallas_call x1, Pallas kernels: 102 us -> 92.2 us  [local(): pl.pallas_call(kernel, out_shape=(out, out), in_specs=[hbm] * 16, out_spe...]
where the time goes in v3:
time: 95.2 us; the launch traced here: 95 us
  Pallas kernels  92.2 us (97%)
  local copies, waits for them, and re-layouts  2.14 us (2%)
    pallas_call x1, Pallas kernels, local(): pl.pallas_call(kernel, out_shape=(out, out), in_specs=[hbm] * 16, out_spe...  92.2 us
    unnamed x4, local copies, waits for them, and re-layouts  2.14 us

profile of v3, /device:TPU:1, one launch (start us, length us, event | category | flops | bytes accessed | tf_op | source)
XLA Modules:
  0.0 95.0 jit_solution(2618980383953858417)
XLA Ops:
  0.6 92.2 %mixer_and_experts.1 = (bf16[256,128]{1,0:T(8,128)(2,1)}, bf16[256,128]{1,0:T(8,128)(2,1)}) custom-call(bf16[256,2048]{1,0:T(8,128)(2,1)} %mix_in.1, bf16[256,2048]{1,0:T(8,128)(2,1)} %moe_in.1, bf16[2048,128]{1,0:T(8,128)(2,1)} %w_x.1, bf16[2048,128]{1,0:T(8,128)(2,1)} %w_y.1, f32[256,128]{1,0:T(8,128)} %shift.1, bf16[1,2048,128]{2,1,0:T(8,128)(2,1)} %w_gate.1, ...), custom_call_target="tpu_custom_call" | custom-call | tf_op jit(solution)/shard_map/mixer_and_experts/pallas_call | solution.py:456
  92.9 0.0 copy-start
  92.9 1.5 %copy.20 = bf16[256,128]{1,0:T(8,128)(2,1)} copy(bf16[256,128]{1,0:T(8,128)(2,1)} %get-tuple-element.4) | data formatting | bytes 131072
  94.4 0.0 copy-done
  94.4 0.6 copy.21
Async XLA Ops:
  92.9 1.5 %copy-start = (bf16[256,128]{1,0:T(8,128)(2,1)S(1)}, bf16[256,128]{1,0:T(8,128)(2,1)}, u32[]{:S(2)}) copy-start(bf16[256,128]{1,0:T(8,128)(2,1)} %get-tuple-element.5) | copy-start | bytes 196612

commit v4 on v3

--- a/solution.py
+++ b/solution.py
@@ -22,24 +22,32 @@
 LANE = 128
 CAP = 32
 SLOTS = EP * CAP
-CHUNKS = 4
+CHUNKS = 8
 CH = SLOTS // CHUNKS
 QROWS = CH // SIDE
 PIECES = 8
 WROWS = D // PIECES
 
-XROWS = [128, 128, 128, 128]
-
-NEAR = [0, 1, -1, 2, -7, 7, 6, 8, 5, -6, -4, -5, 4, -3, 3, -2]
+XROWS = [64, 96, 96, 64, 64, 32, 64, 96]
+
+NEAR = [0, -1, 2, 1, 8, -7, -6, 7, -4, 5, 6, -5, 3, -3, 4, -2]
 PLACE = {off % RING: at for at, off in enumerate(NEAR)}
 
+def place_of(at, c):
+    n = at % SIDE
+    return at // SIDE * 2 * SIDE + (c + n) % 2 * SIDE + n
+
+
 ORDER = [
-    "MA0", "Y10", "X10", "W16", "Y20", "X20", "Y30", "W21", "X30", "MB0", "MC0", "Y11", "X11", "Y40", "X40", "Y12",
-    "X12", "Y21", "X21", "Y22", "Y31", "X22", "Y13", "X13", "X31", "Y32", "Y23", "Y41", "X32", "X23", "UP0", "X41",
-    "MD0", "Y33", "Y42", "W17", "W20", "X42", "X33", "B10", "UP1", "Y43", "W23", "B20", "UP2", "X43", "W22", "B11",
-    "B12", "UP3", "B21", "DN0", "B13", "B22", "DN1", "B23", "DN2", "DN3",
+    "MA0", "W10", "W11", "W12", "Y10", "Y11", "X10", "X11", "W14", "Y20", "Y21", "W15", "X21", "X20", "W16", "Y30",
+    "MB0", "MC0", "X31", "Y31", "W20", "X30", "X12", "X13", "Y40", "Y12", "Y13", "Y41", "X15", "Y15", "X14", "Y14",
+    "X17", "X41", "X16", "X22", "X23", "Y16", "W21", "X40", "Y23", "Y22", "Y17", "X25", "Y25", "X24", "Y24", "W22",
+    "X32", "UP1", "X27", "X26", "UP0", "Y32", "X33", "Y33", "MD0", "X34", "Y34", "X42", "Y42", "Y35", "X35", "X43",
+    "X36", "Y43", "Y44", "UP2", "X44", "X45", "W17", "Y26", "X37", "Y45", "UP3", "X46", "UP4", "Y36", "Y27", "B10",
+    "B12", "B11", "W23", "UP5", "X47", "Y37", "B13", "B20", "Y46", "B22", "B14", "B21", "Y47", "B15", "DN0", "B23",
+    "DN2", "UP6", "B24", "DN1", "UP7", "B25", "DN3", "DN4", "B16", "DN5", "B17", "B26", "B27", "DN6", "DN7",
 ]
-EARLY = 6
+EARLY = [3]
 
 
 def softplus(v):
@@ -84,8 +92,8 @@
             got = jnp.where(of == n, values[n], got)
         return got
 
-    def offset(k, of):
-        return by_x(NEAR[SIDE * k : SIDE * (k + 1)], of)
+    def offset(m, of):
+        return by_x(NEAR[SIDE * m : SIDE * (m + 1)], of)
 
     def lanes(n):
         return pl.ds(pl.multiple_of(n * LANE, LANE), LANE)
@@ -115,19 +123,20 @@
     def greet(where):
         pl.semaphore_signal(barrier, inc=1, device_id=where, device_id_type=MESH)
 
-    for where in plane + row[2:]:
-        greet(where)
-    greet((peer(0, 1 - core), tp))
-    for at in range(1, RING):
+    far = sorted(range(1, RING), key=lambda at: -abs(NEAR[at]))
+    for at in far:
         for c in range(CORES):
             greet((peer(at, c), tp))
-    for k in range(CHUNKS):
+    for m in sorted(range(RING // SIDE), key=lambda m: -max(map(abs, NEAR[SIDE * m : SIDE * (m + 1)]))):
         for by in range(1, SIDE):
             other = wrap(x + by, SIDE)
             for c in range(CORES):
-                greet((wrap(z + offset(k, x), RING) * CORES + c, y * SIDE + other))
-                greet((wrap(z - offset(k, other), RING) * CORES + c, y * SIDE + other))
-    greeted = len(plane) + 1 + EP - 1 + 2 * CHUNKS * (SIDE - 1) * CORES
+                greet((wrap(z + offset(m, x), RING) * CORES + c, y * SIDE + other))
+                greet((wrap(z - offset(m, other), RING) * CORES + c, y * SIDE + other))
+    greet((peer(0, 1 - core), tp))
+    for where in plane + row[2:]:
+        greet(where)
+    greeted = len(plane) + 1 + EP - 1 + 2 * RING // SIDE * (SIDE - 1) * CORES
 
     pending = []
 
@@ -165,11 +174,17 @@
     at = jnp.zeros((1, LANE), jnp.int32)
     for n in range(1, RING):
         at = jnp.where(off == NEAR[n] % RING, n, at)
-    base = (CAP * (CORES * at + lane_1 % CORES)).astype(F32)
+    base = (CAP * place_of(at, lane_1 % CORES)).astype(F32)
     slot_lane = lax.broadcasted_iota(jnp.int32, (ROWS, SLOTS), 1)
     for ref, hot, r in zip((c0, c1), onehot, rank):
         slot = jnp.sum(hot.astype(F32) * (r + base), axis=1, keepdims=True).astype(jnp.int32)
         ref[...] = jnp.where(slot_lane == slot, 1.0, 0.0).astype(BF16)
+
+    loaded("moe", "moe_gain")
+    own_rows = normed(moe_v, moe_gain_v, lanes(tp))
+    sent[...] = lax.dot_general(
+        c0[...] + c1[...], own_rows, (((0,), (0,)), ((), ())), preferred_element_type=F32
+    ).astype(BF16).reshape(EP, CAP, LANE)
 
     with jax.named_scope("barrier"):
         pl.semaphore_wait(barrier, greeted)
@@ -189,21 +204,15 @@
         for n, (view, slot) in enumerate(views):
             ways["W", step, q, n] = launch(view, view, w_send.at[2 * slot + n], w_recv.at[2 * slot + n], row[n])
 
-    for q in range(EARLY):
+    for q in EARLY:
         weights(1, q)
-
-    loaded("moe", "moe_gain")
-    own_rows = normed(moe_v, moe_gain_v, lanes(tp))
-    sent[...] = lax.dot_general(
-        c0[...] + c1[...], own_rows, (((0,), (0,)), ((), ())), preferred_element_type=F32
-    ).astype(BF16).reshape(EP, CAP, LANE)
 
     def block(buf, p):
         return buf.at[y, x, pl.ds(pl.multiple_of(p * CAP, CAP), CAP)]
 
     def dispatch(at, c):
-        local = CORES * PLACE[-NEAR[at] % RING] + c
-        place = CORES * at + core
+        local = place_of(PLACE[-NEAR[at] % RING], c)
+        place = place_of(at, core)
         where = wrap(z - NEAR[at], RING) * CORES + c
         launch(sent.at[local], block(X, place), d_send.at[local], d_recv.at[place], (where, tp))
 
@@ -211,8 +220,8 @@
     for at in range(1, RING):
         for c in range(CORES):
             dispatch(at, c)
-    own = pl.ds(pl.multiple_of(core * CAP, CAP), CAP)
-    X[y, x, own, :] = sent[core]
+    mine = place_of(0, core)
+    X[y, x, pl.ds(pl.multiple_of(mine * CAP, CAP), CAP), :] = sent[mine]
 
     def arrived(p, sem, ref):
         pltpu.make_async_remote_copy(
@@ -225,15 +234,20 @@
             return
         ways["in", k] = None
         for p in range(k * CH // CAP, (k + 1) * CH // CAP):
-            if p >= CORES:
+            if p % SIDE or k > 1:
                 arrived(p, d_recv, block(X, p))
-            elif p == 0:
-                arrived(1 - core, d_recv, block(X, 1 - core))
+            else:
+
+                @pl.when(mine != p)
+                def _():
+                    arrived(p, d_recv, block(X, p))
 
     def gather(part, step, k):
         lo, size = k * CH, XROWS[k]
         if part == "Y":
             lo, size = lo + size, CH - size
+        if size == 0:
+            return
         full, first, second = pl.ds(lo, size), pl.ds(lo, size // 2), pl.ds(lo + size // 2, size // 2)
         along_x = (part == "X") == (step < 3)
         if step == 1:
@@ -271,17 +285,18 @@
     def run_up(k):
         for part in "XY":
             for n in range(2):
-                ways[part, 4, k, n].wait_recv()
-        if k == 0:
-            loaded("gate", "up")
+                if (part, 4, k, n) in ways:
+                    ways[part, 4, k, n].wait_recv()
+        if "up" not in ways:
+            ways["up"] = loaded("gate", "up")
         both = jnp.dot(all_blocks(X, pl.ds(k * CH, CH)), gu_v[...], preferred_element_type=F32)
         g, u = both[:, :LANE], both[:, LANE:]
         hown[pl.ds(k * CH, CH), :] = (g * jax.nn.sigmoid(g) * u).astype(BF16)
-        mine = pl.ds(k * QROWS, QROWS)
+        ours = pl.ds(k * QROWS, QROWS)
         for n, who in enumerate((east, west, across)):
             slot = 3 * k + n
-            ways["A", k, n] = launch(hown.at[quarter(k, who)], H.at[y, x, mine], a_send.at[slot], a_recv.at[slot], row[n])
-        H[y, x, mine, :] = hown[quarter(k, x), :]
+            ways["A", k, n] = launch(hown.at[quarter(k, who)], H.at[y, x, ours], a_send.at[slot], a_recv.at[slot], row[n])
+        H[y, x, ours, :] = hown[quarter(k, x), :]
 
     def spread(step, k):
         slot = 4 * k + 2 * (step - 1)
@@ -297,17 +312,16 @@
                 ways["B", 1, k, n].wait_recv()
             ways["B", step, k, n] = launch(views[n], views[n], b_send.at[slot + n], b_recv.at[slot + n], plane[2 + n])
 
-    def give(k, c, by, act):
-        other = wrap(x + by, SIDE)
-        off = offset(k, x)
-        place = by_x([PLACE[-v % RING] for v in NEAR[SIDE * k : SIDE * (k + 1)]], x) * CORES + core
-        slot = (k * CORES + c) * SIDE + by
+    def give(k, by, act):
+        other, m = wrap(x + by, SIDE), k // 2
+        place = by_x([place_of(PLACE[-v % RING], core) for v in NEAR[SIDE * m : SIDE * (m + 1)]], x)
+        slot = k * SIDE + by
         copy = pltpu.make_async_remote_copy(
-            src_ref=res.at[k * CORES + c, other], dst_ref=ret.at[place], send_sem=r_send.at[slot], recv_sem=r_recv.at[place],
-            device_id=(wrap(z + off, RING) * CORES + c, y * SIDE + other), device_id_type=MESH,
+            src_ref=res.at[k, other], dst_ref=ret.at[place], send_sem=r_send.at[slot], recv_sem=r_recv.at[place],
+            device_id=(wrap(z + offset(m, x), RING) * CORES + (x + k) % CORES, y * SIDE + other), device_id_type=MESH,
         )
-        if k == 0 and by == 0:
-            stays = jnp.logical_and(x == 0, core == c)
+        if k < CORES and by == 0:
+            stays = jnp.logical_and(x == 0, core == k)
 
             @pl.when(jnp.logical_not(stays))
             def _():
@@ -317,7 +331,7 @@
 
                 @pl.when(stays)
                 def _():
-                    ret[core] = res[c, 0]
+                    ret[mine] = res[k, 0]
 
         else:
             act(copy)
@@ -328,7 +342,8 @@
     def run_down(k):
         for n in range(2):
             ways["B", 2, k, n].wait_recv()
-        if k == 0:
+        if "down" not in ways:
+            ways["down"] = None
             for q in range(PIECES // 2):
                 ways["W", 1, q, 1].wait_recv()
                 ways["W", 1, q + PIECES // 2, 0].wait_recv()
@@ -336,11 +351,9 @@
                 ways["W", 2, q, 1].wait_recv()
         out = jnp.dot(all_blocks(H, pl.ds(k * QROWS, QROWS)), wd[...], preferred_element_type=F32).astype(BF16)
         for n in range(SIDE):
-            for c in range(CORES):
-                res[k * CORES + c, n] = out[c * CAP : (c + 1) * CAP, n * LANE : (n + 1) * LANE]
+            res[k, n] = out[:, n * LANE : (n + 1) * LANE]
         for by in range(SIDE):
-            for c in range(CORES):
-                give(k, c, by, starts)
+            give(k, by, starts)
 
     def mix_a():
         loaded("mix", "mix_gain", "w_x", "w_y")
@@ -404,7 +417,7 @@
         mixer_out[...] = (lru * jax.nn.gelu(ybr[...].astype(F32), approximate=True)).astype(BF16)
 
     for item in ORDER:
-        what, k = item[:-1], int(item[-1])
+        what, k = item[:2], int(item[2:])
         with jax.named_scope(f"{what}_{k}"):
             if what == "UP":
                 run_up(k)
@@ -419,29 +432,34 @@
             else:
                 gather(what[0], int(what[1]), k)
 
-    with jax.named_scope("back"):
-        arrived(1 - core, r_recv, ret.at[1 - core])
-        for p in range(CORES, EP):
-            arrived(p, r_recv, ret.at[p])
-
-        @pl.when(x != 0)
-        def _():
-            arrived(core, r_recv, ret.at[core])
-
-    back = ret[...].reshape(SLOTS, LANE)
-    loaded("weight")
-    w = columns(weight_v)
-    total = w[:, 0:1] + w[:, 1:2]
-    out = w[:, 0:1] / total * jnp.dot(c0[...], back, preferred_element_type=F32)
-    out = out + w[:, 1:2] / total * jnp.dot(c1[...], back, preferred_element_type=F32)
-    moe_out[...] = out.astype(BF16)
     with jax.named_scope("sends"):
         for copy in pending:
             copy.wait_send()
         for k in range(CHUNKS):
             for by in range(SIDE):
-                for c in range(CORES):
-                    give(k, c, by, lambda copy: copy.wait_send())
+                give(k, by, lambda copy: copy.wait_send())
+    loaded("weight")
+    w = columns(weight_v)
+    total = w[:, 0:1] + w[:, 1:2]
+    picked = [jnp.zeros((ROWS, LANE), F32)] * 2
+    for half in range(2):
+        blocks = range(half * EP // 2, (half + 1) * EP // 2)
+        with jax.named_scope(f"back_{half}"):
+            for p in blocks:
+                if p not in (0, SIDE):
+                    arrived(p, r_recv, ret.at[p])
+            if half == 0:
+                arrived(SIDE - mine, r_recv, ret.at[SIDE - mine])
+
+                @pl.when(x != 0)
+                def _():
+                    arrived(mine, r_recv, ret.at[mine])
+
+        part = pl.ds(half * SLOTS // 2, SLOTS // 2)
+        back = ret[pl.ds(half * EP // 2, EP // 2)].reshape(SLOTS // 2, LANE)
+        for n, ref in enumerate((c0, c1)):
+            picked[n] = picked[n] + jnp.dot(ref[:, part], back, preferred_element_type=F32)
+    moe_out[...] = (w[:, 0:1] / total * picked[0] + w[:, 1:2] / total * picked[1]).astype(BF16)
 
 
 def local(
@@ -465,7 +483,7 @@
             v((1, D), F32), v((2, ROWS), jnp.int32), v((2, ROWS), F32),
             v((ROWS, SLOTS), BF16), v((ROWS, SLOTS), BF16), v((EP, CAP, LANE), BF16),
             v((SIDE, SIDE, SLOTS, LANE), BF16), v((SLOTS, LANE), BF16), v((SIDE, SIDE, SLOTS // SIDE, LANE), BF16),
-            v((CHUNKS * CORES, SIDE, CAP, LANE), BF16), v((EP, CAP, LANE), BF16),
+            v((CHUNKS, SIDE, CAP, LANE), BF16), v((EP, CAP, LANE), BF16),
             v((ROWS, LANE), BF16), v((ROWS + 8, LANE), F32), v((ROWS, LANE), BF16),
             v((16, LANE), BF16), v((16, LANE), BF16), v((ROWS, LANE), F32), v((ROWS, LANE), F32),
             v((2, LANE), F32), v((EP, 2, LANE), F32),

time: 95.2 us -> 90.2 us (0.947)
  Pallas kernels: 92.2 us -> 87.2 us
    pallas_call x1, Pallas kernels: 92.2 us -> 87.2 us  [local(): pl.pallas_call(kernel, out_shape=(out, out), in_specs=[hbm] * 16, out_spe...]
where the time goes in v4:
time: 90.2 us; the launch traced here: 90 us
  Pallas kernels  87.2 us (97%)
  local copies, waits for them, and re-layouts  2.14 us (2%)
    pallas_call x1, Pallas kernels, local(): pl.pallas_call(kernel, out_shape=(out, out), in_specs=[hbm] * 16, out_spe...  87.2 us
    unnamed x4, local copies, waits for them, and re-layouts  2.14 us

profile of v4, /device:TPU:1, one launch (start us, length us, event | category | flops | bytes accessed | tf_op | source)
XLA Modules:
  0.0 90.0 jit_solution(4576191773862230479)
XLA Ops:
  0.6 87.2 %mixer_and_experts.1 = (bf16[256,128]{1,0:T(8,128)(2,1)}, bf16[256,128]{1,0:T(8,128)(2,1)}) custom-call(bf16[256,2048]{1,0:T(8,128)(2,1)} %mix_in.1, bf16[256,2048]{1,0:T(8,128)(2,1)} %moe_in.1, bf16[2048,128]{1,0:T(8,128)(2,1)} %w_x.1, bf16[2048,128]{1,0:T(8,128)(2,1)} %w_y.1, f32[256,128]{1,0:T(8,128)} %shift.1, bf16[1,2048,128]{2,1,0:T(8,128)(2,1)} %w_gate.1, ...), custom_call_target="tpu_custom_call" | custom-call | tf_op jit(solution)/shard_map/mixer_and_experts/pallas_call | solution.py:474
  87.9 0.0 copy-start
  87.9 1.5 %copy.20 = bf16[256,128]{1,0:T(8,128)(2,1)} copy(bf16[256,128]{1,0:T(8,128)(2,1)} %get-tuple-element.4) | data formatting | bytes 131072
  89.4 0.0 copy-done
  89.4 0.6 copy.21
Async XLA Ops:
  87.9 1.5 %copy-start = (bf16[256,128]{1,0:T(8,128)(2,1)S(1)}, bf16[256,128]{1,0:T(8,128)(2,1)}, u32[]{:S(2)}) copy-start(bf16[256,128]{1,0:T(8,128)(2,1)} %get-tuple-element.5) | copy-start | bytes 196612

commit v5 on v4

--- a/solution.py
+++ b/solution.py
@@ -28,7 +28,7 @@
 PIECES = 8
 WROWS = D // PIECES
 
-XROWS = [64, 96, 96, 64, 64, 32, 64, 96]
+XROWS = [128, 128, 64, 64, 64, 64, 64, 64]
 
 NEAR = [0, -1, 2, 1, 8, -7, -6, 7, -4, 5, 6, -5, 3, -3, 4, -2]
 PLACE = {off % RING: at for at, off in enumerate(NEAR)}
@@ -38,16 +38,20 @@
     return at // SIDE * 2 * SIDE + (c + n) % 2 * SIDE + n
 
 
+STRAIGHT = []
+
+FINE = [0, 1]
+
 ORDER = [
-    "MA0", "W10", "W11", "W12", "Y10", "Y11", "X10", "X11", "W14", "Y20", "Y21", "W15", "X21", "X20", "W16", "Y30",
-    "MB0", "MC0", "X31", "Y31", "W20", "X30", "X12", "X13", "Y40", "Y12", "Y13", "Y41", "X15", "Y15", "X14", "Y14",
-    "X17", "X41", "X16", "X22", "X23", "Y16", "W21", "X40", "Y23", "Y22", "Y17", "X25", "Y25", "X24", "Y24", "W22",
-    "X32", "UP1", "X27", "X26", "UP0", "Y32", "X33", "Y33", "MD0", "X34", "Y34", "X42", "Y42", "Y35", "X35", "X43",
-    "X36", "Y43", "Y44", "UP2", "X44", "X45", "W17", "Y26", "X37", "Y45", "UP3", "X46", "UP4", "Y36", "Y27", "B10",
-    "B12", "B11", "W23", "UP5", "X47", "Y37", "B13", "B20", "Y46", "B22", "B14", "B21", "Y47", "B15", "DN0", "B23",
-    "DN2", "UP6", "B24", "DN1", "UP7", "B25", "DN3", "DN4", "B16", "DN5", "B17", "B26", "B27", "DN6", "DN7",
+    "MA0", "W11", "W12", "W13", "Xa0", "Xa1", "X11", "X10", "W15", "Xd0", "W16", "Xd1", "Xb1", "X21", "X20", "Xb0",
+    "W17", "MB0", "W21", "MC0", "Xc1", "W22", "Xc0", "Xe1", "Y12", "X12", "X13", "Xe0", "W23", "Y13", "Xf1", "Y14",
+    "X14", "Y15", "X15", "Xf0", "X16", "Y17", "X17", "Y16", "X22", "Y22", "X23", "W14", "Y23", "UP1", "Y24", "X24",
+    "Y25", "X25", "UP0", "X26", "Y27", "X27", "X32", "Y32", "Y26", "X33", "Y33", "MD0", "X34", "Y34", "B10", "Y35",
+    "B11", "X42", "Y42", "X43", "Y43", "X35", "Y36", "B20", "Y44", "X44", "Y45", "B21", "X36", "UP2", "Y37", "UP3",
+    "X37", "Y46", "X45", "UP4", "W20", "B12", "X46", "Y47", "X47", "B13", "UP5", "B14", "B22", "DN0", "DN1", "UP6",
+    "UP7", "B23", "B24", "B15", "DN2", "B16", "DN3", "B17", "DN4", "B25", "B26", "B27", "DN5", "DN6", "DN7",
 ]
-EARLY = [3]
+EARLY = [0]
 
 
 def softplus(v):
@@ -70,7 +74,7 @@
     mix_v, moe_v, win_v, shift_v, gu_v, wd,
     mix_gain_v, conv_taps_v, recur_v, input_v, logit_v, moe_gain_v, routes_v, weight_v,
     c0, c1, sent, X, hown, H, res, ret, ybr, xb, xcv, halo_out, halo_in, sa, sb, carry_out, carry_in,
-    load_sem, x_send, x_recv, b_send, b_recv, a_send, a_recv, w_send, w_recv,
+    load_sem, x_send, x_recv, b_send, b_recv, a_send, a_recv, w_send, w_recv, f_send, f_recv,
     d_send, d_recv, r_send, r_recv, k_send, k_recv, h_sem,
 ):
     ep, tp = lax.axis_index("ep"), lax.axis_index("tp")
@@ -85,6 +89,7 @@
     across = wrap(x + 2, SIDE)
     plane = [(ep, y * SIDE + east), (ep, y * SIDE + west), (ep, north * SIDE + x), (ep, south * SIDE + x)]
     row = [plane[0], plane[1], (ep, y * SIDE + across)]
+    others = [(dx, wrap(y + dy, SIDE)) for dy in range(SIDE) for dx in range(SIDE) if dx or dy]
 
     def by_x(values, of):
         got = values[0]
@@ -134,9 +139,9 @@
                 greet((wrap(z + offset(m, x), RING) * CORES + c, y * SIDE + other))
                 greet((wrap(z - offset(m, other), RING) * CORES + c, y * SIDE + other))
     greet((peer(0, 1 - core), tp))
-    for where in plane + row[2:]:
-        greet(where)
-    greeted = len(plane) + 1 + EP - 1 + 2 * RING // SIDE * (SIDE - 1) * CORES
+    for dx, its_y in others:
+        greet((ep, its_y * SIDE + wrap(x + dx, SIDE)))
+    greeted = len(others) + EP - 1 + 2 * RING // SIDE * (SIDE - 1) * CORES
 
     pending = []
 
@@ -189,14 +194,19 @@
     with jax.named_scope("barrier"):
         pl.semaphore_wait(barrier, greeted)
     loaded("down")
-    ways = {}
+    ways, got = {}, set()
+
+    def received(*key):
+        if key not in got:
+            got.add(key)
+            ways[key].wait_recv()
 
     def weights(step, q):
         if step == 1:
             views = [(wd.at[pl.ds(q * WROWS, WROWS), lanes(x)], q)] * 2
         else:
-            ways["W", 1, q, 0].wait_recv()
-            ways["W", 1, q + PIECES // 2, 1].wait_recv()
+            received("W", 1, q, 0)
+            received("W", 1, q + PIECES // 2, 1)
             views = [
                 (wd.at[pl.ds(q * WROWS, WROWS), lanes(west)], PIECES + q),
                 (wd.at[pl.ds((q + PIECES // 2) * WROWS, WROWS), lanes(east)], PIECES + q),
@@ -267,15 +277,35 @@
             views = [X.at[south, :, first], X.at[north, :, second]]
         if step == 3:
             for n in range(2):
-                ways[part, 2, k, n].wait_recv()
+                received(part, 2, k, n)
         for n in range(2):
             if step == 2 or step == 4:
-                ways[part, step - 1, k, n].wait_recv()
+                received(part, step - 1, k, n)
             slot = ((("XY".index(part) * CHUNKS) + k) * 4 + step - 1) * 2 + n
             ways[part, step, k, n] = launch(
                 views[n], views[n], x_send.at[slot], x_recv.at[slot], plane[n if along_x else 2 + n]
             )
 
+    def fine(letter, k):
+        lo = k * CH
+        full, first, second = pl.ds(lo, CH), pl.ds(lo, CH // 2), pl.ds(lo + CH // 2, CH // 2)
+        stage, at = divmod("abcdef".index(letter), 3)
+        cols = ([x], [west, east], [across])[at]
+        if letter == "a":
+            await_dispatch(k)
+        for step in range(1, at + 1 if stage == 0 else 1):
+            for n in range(2):
+                received("X", step, k, n)
+        for i, col in enumerate(cols):
+            for n in range(2):
+                if stage == 0:
+                    view = X.at[y, col, full]
+                else:
+                    received("F", "abc"[at], k, i, n)
+                    view = X.at[south, col, first] if n == 0 else X.at[north, col, second]
+                slot = (FINE.index(k) * 6 + "abcdef".index(letter)) * 4 + 2 * i + n
+                ways["F", letter, k, i, n] = launch(view, view, f_send.at[slot], f_recv.at[slot], plane[2 + n])
+
     def all_blocks(buf, rows):
         return jnp.concatenate([buf[a, b, rows, :] for a in range(SIDE) for b in range(SIDE)], axis=1)
 
@@ -286,14 +316,23 @@
         for part in "XY":
             for n in range(2):
                 if (part, 4, k, n) in ways:
-                    ways[part, 4, k, n].wait_recv()
+                    received(part, 4, k, n)
+        for key in [key for key in ways if key[0] == "F" and key[1] in "def" and key[2] == k]:
+            received(*key)
         if "up" not in ways:
             ways["up"] = loaded("gate", "up")
         both = jnp.dot(all_blocks(X, pl.ds(k * CH, CH)), gu_v[...], preferred_element_type=F32)
         g, u = both[:, :LANE], both[:, LANE:]
         hown[pl.ds(k * CH, CH), :] = (g * jax.nn.sigmoid(g) * u).astype(BF16)
         ours = pl.ds(k * QROWS, QROWS)
-        for n, who in enumerate((east, west, across)):
+        if k in STRAIGHT:
+            for n, (dx, its_y) in enumerate(others):
+                slot = 3 * CHUNKS + STRAIGHT.index(k) * len(others) + n
+                who = wrap(x + dx, SIDE)
+                ways["S", k, n] = launch(
+                    hown.at[quarter(k, who)], H.at[y, x, ours], a_send.at[slot], a_recv.at[slot], (ep, its_y * SIDE + who)
+                )
+        for n, who in enumerate(() if k in STRAIGHT else (east, west, across)):
             slot = 3 * k + n
             ways["A", k, n] = launch(hown.at[quarter(k, who)], H.at[y, x, ours], a_send.at[slot], a_recv.at[slot], row[n])
         H[y, x, ours, :] = hown[quarter(k, x), :]
@@ -303,13 +342,13 @@
         lo = k * QROWS
         if step == 1:
             for n, who in enumerate((west, east, across)):
-                ways["A", k, n].wait_recv()
+                received("A", k, n)
             views = [H.at[y, :, pl.ds(lo, QROWS)]] * 2
         else:
             views = [H.at[south, :, pl.ds(lo, QROWS // 2)], H.at[north, :, pl.ds(lo + QROWS // 2, QROWS // 2)]]
         for n in range(2):
             if step == 2:
-                ways["B", 1, k, n].wait_recv()
+                received("B", 1, k, n)
             ways["B", step, k, n] = launch(views[n], views[n], b_send.at[slot + n], b_recv.at[slot + n], plane[2 + n])
 
     def give(k, by, act):
@@ -340,15 +379,18 @@
         copy.start()
 
     def run_down(k):
-        for n in range(2):
-            ways["B", 2, k, n].wait_recv()
+        if k in STRAIGHT:
+            for n in range(len(others)):
+                received("S", k, n)
+        for n in range(0 if k in STRAIGHT else 2):
+            received("B", 2, k, n)
         if "down" not in ways:
             ways["down"] = None
             for q in range(PIECES // 2):
-                ways["W", 1, q, 1].wait_recv()
-                ways["W", 1, q + PIECES // 2, 0].wait_recv()
-                ways["W", 2, q, 0].wait_recv()
-                ways["W", 2, q, 1].wait_recv()
+                received("W", 1, q, 1)
+                received("W", 1, q + PIECES // 2, 0)
+                received("W", 2, q, 0)
+                received("W", 2, q, 1)
         out = jnp.dot(all_blocks(H, pl.ds(k * QROWS, QROWS)), wd[...], preferred_element_type=F32).astype(BF16)
         for n in range(SIDE):
             res[k, n] = out[:, n * LANE : (n + 1) * LANE]
@@ -362,10 +404,10 @@
         ybr[...] = both[:, LANE:]
         xb[pl.ds(8, ROWS), :] = both[:, :LANE].astype(F32)
         halo_out[...] = both[ROWS - 16 :, :LANE]
-        ways["halo"] = launch(halo_out, halo_in, h_sem.at[0], h_sem.at[1], (wrap(ep + 1, EP), tp))
+        ways["halo",] = launch(halo_out, halo_in, h_sem.at[0], h_sem.at[1], (wrap(ep + 1, EP), tp))
 
     def mix_b():
-        ways["halo"].wait_recv()
+        received("halo")
         loaded("taps", "recur", "input", "logit", "shift")
         xb[pl.ds(0, 8), :] = jnp.where(ep > 0, halo_in[...].astype(F32)[8:], 0.0)
         conv = jnp.zeros((ROWS, LANE), F32)
@@ -429,6 +471,8 @@
                 weights(int(what[1]), k)
             elif what[0] == "B":
                 spread(int(what[1]), k)
+            elif what[1] in "abcdef":
+                fine(what[1], k)
             else:
                 gather(what[0], int(what[1]), k)
 
@@ -471,6 +515,8 @@
     dma = pltpu.SemaphoreType.DMA
     out = jax.ShapeDtypeStruct((ROWS, LANE), BF16)
     v = pltpu.VMEM
+    fines = 24 * len(FINE)
+    straight = CHUNKS * 3 + len(STRAIGHT) * (SIDE * SIDE - 1)
     return pl.pallas_call(
         kernel,
         out_shape=(out, out),
@@ -488,7 +534,7 @@
             v((16, LANE), BF16), v((16, LANE), BF16), v((ROWS, LANE), F32), v((ROWS, LANE), F32),
             v((2, LANE), F32), v((EP, 2, LANE), F32),
             dma((16,)), dma((CHUNKS * 16,)), dma((CHUNKS * 16,)), dma((CHUNKS * 4,)), dma((CHUNKS * 4,)),
-            dma((CHUNKS * 3,)), dma((CHUNKS * 3,)), dma((PIECES * 3,)), dma((PIECES * 3,)), dma((EP,)), dma((EP,)),
+            dma((straight,)), dma((straight,)), dma((PIECES * 3,)), dma((PIECES * 3,)), dma((fines,)), dma((fines,)), dma((EP,)), dma((EP,)),
             dma((EP,)), dma((EP,)), dma((EP,)), dma((EP,)), dma((2,)),
         ],
         compiler_params=pltpu.CompilerParams(

time: 90.2 us -> 89.3 us (0.990)
  no operation moved by 1% of the time
where the time goes in v5:
time: 89.3 us; the launch traced here: 89.1 us
  Pallas kernels  86.3 us (97%)
  local copies, waits for them, and re-layouts  2.14 us (2%)
    pallas_call x1, Pallas kernels, local(): pl.pallas_call(kernel, out_shape=(out, out), in_specs=[hbm] * 16, out_spe...  86.3 us
    unnamed x4, local copies, waits for them, and re-layouts  2.14 us

profile of v5, /device:TPU:1, one launch (start us, length us, event | category | flops | bytes accessed | tf_op | source)
XLA Modules:
  0.0 89.1 jit_solution(5102779981750087329)
XLA Ops:
  0.6 86.3 %mixer_and_experts.1 = (bf16[256,128]{1,0:T(8,128)(2,1)}, bf16[256,128]{1,0:T(8,128)(2,1)}) custom-call(bf16[256,2048]{1,0:T(8,128)(2,1)} %mix_in.1, bf16[256,2048]{1,0:T(8,128)(2,1)} %moe_in.1, bf16[2048,128]{1,0:T(8,128)(2,1)} %w_x.1, bf16[2048,128]{1,0:T(8,128)(2,1)} %w_y.1, f32[256,128]{1,0:T(8,128)} %shift.1, bf16[1,2048,128]{2,1,0:T(8,128)(2,1)} %w_gate.1, ...), custom_call_target="tpu_custom_call" | custom-call | tf_op jit(solution)/shard_map/mixer_and_experts/pallas_call | solution.py:520
  87.0 0.0 copy-start
  87.0 1.5 %copy.20 = bf16[256,128]{1,0:T(8,128)(2,1)} copy(bf16[256,128]{1,0:T(8,128)(2,1)} %get-tuple-element.4) | data formatting | bytes 131072
  88.5 0.0 copy-done
  88.5 0.6 copy.21
Async XLA Ops:
  87.0 1.5 %copy-start = (bf16[256,128]{1,0:T(8,128)(2,1)S(1)}, bf16[256,128]{1,0:T(8,128)(2,1)}, u32[]{:S(2)}) copy-start(bf16[256,128]{1,0:T(8,128)(2,1)} %get-tuple-element.5) | copy-start | bytes 196612

commit v6 on v5

--- a/solution.py
+++ b/solution.py
@@ -70,7 +70,7 @@
 def kernel(
     mix_in, moe_in, w_x, w_y, shift, w_gate, w_up, w_down,
     mix_gain, conv_taps, recur_w, input_w, logit, moe_gain, routes, weight,
-    mixer_out, moe_out,
+    both_out,
     mix_v, moe_v, win_v, shift_v, gu_v, wd,
     mix_gain_v, conv_taps_v, recur_v, input_v, logit_v, moe_gain_v, routes_v, weight_v,
     c0, c1, sent, X, hown, H, res, ret, ybr, xb, xcv, halo_out, halo_in, sa, sb, carry_out, carry_in,
@@ -456,7 +456,7 @@
             pair = carry_in[e]
             state = jnp.where(e < ep, pair[0:1] * state + pair[1:2], state)
         lru = sb[...] + sa[...] * state
-        mixer_out[...] = (lru * jax.nn.gelu(ybr[...].astype(F32), approximate=True)).astype(BF16)
+        both_out[0] = (lru * jax.nn.gelu(ybr[...].astype(F32), approximate=True)).astype(BF16)
 
     for item in ORDER:
         what, k = item[:2], int(item[2:])
@@ -503,7 +503,7 @@
         back = ret[pl.ds(half * EP // 2, EP // 2)].reshape(SLOTS // 2, LANE)
         for n, ref in enumerate((c0, c1)):
             picked[n] = picked[n] + jnp.dot(ref[:, part], back, preferred_element_type=F32)
-    moe_out[...] = (w[:, 0:1] / total * picked[0] + w[:, 1:2] / total * picked[1]).astype(BF16)
+    both_out[1] = (w[:, 0:1] / total * picked[0] + w[:, 1:2] / total * picked[1]).astype(BF16)
 
 
 def local(
@@ -513,15 +513,15 @@
     hbm = pl.BlockSpec(memory_space=pltpu.HBM)
     vmem = pl.BlockSpec(memory_space=pltpu.VMEM)
     dma = pltpu.SemaphoreType.DMA
-    out = jax.ShapeDtypeStruct((ROWS, LANE), BF16)
+    out = jax.ShapeDtypeStruct((2, ROWS, LANE), BF16)
     v = pltpu.VMEM
     fines = 24 * len(FINE)
     straight = CHUNKS * 3 + len(STRAIGHT) * (SIDE * SIDE - 1)
-    return pl.pallas_call(
+    both = pl.pallas_call(
         kernel,
-        out_shape=(out, out),
+        out_shape=out,
         in_specs=[hbm] * 16,
-        out_specs=(vmem, vmem),
+        out_specs=vmem,
         scratch_shapes=[
             v((ROWS, D), BF16), v((ROWS, D), BF16), v((D, 2 * LANE), BF16), v((ROWS, LANE), F32),
             v((D, 2 * LANE), BF16), v((D, SIDE * LANE), BF16),
@@ -546,6 +546,7 @@
         mix_gain.reshape(1, D), conv_taps, recur_gate_w, input_gate_w, decay_logit.reshape(1, LANE),
         moe_gain.reshape(1, D), routes.T, route_weight.T,
     )
+    return both[0], both[1]
 
 
 def solution(mesh):

time: 89.3 us -> 88.7 us (level)
    unnamed x4 -> x0, local copies, waits for them, and re-layouts: 2.14 us -> none
    squeeze x0 -> x1, local copies, waits for them, and re-layouts: none -> 1.53 us  [local(): return (both[0], both[1])]
where the time goes in v6:
time: 88.7 us; the launch traced here: 88.6 us
  Pallas kernels  86.4 us (97%)
  local copies, waits for them, and re-layouts  1.53 us (2%)
    pallas_call x1, Pallas kernels, local(): pl.pallas_call(kernel, out_shape=out, in_specs=[hbm] * 16, out_specs=vmem...  86.4 us

profile of v6, /device:TPU:1, one launch (start us, length us, event | category | flops | bytes accessed | tf_op | source)
XLA Modules:
  0.0 88.6 jit_solution(6996361618055959961)
XLA Ops:
  0.6 86.4 %mixer_and_experts.1 = bf16[2,256,128]{2,1,0:T(8,128)(2,1)} custom-call(bf16[256,2048]{1,0:T(8,128)(2,1)} %mix_in.1, bf16[256,2048]{1,0:T(8,128)(2,1)} %moe_in.1, bf16[2048,128]{1,0:T(8,128)(2,1)} %w_x.1, bf16[2048,128]{1,0:T(8,128)(2,1)} %w_y.1, f32[256,128]{1,0:T(8,128)} %shift.1, bf16[1,2048,128]{2,1,0:T(8,128)(2,1)} %w_gate.1, ...), custom_call_target="tpu_custom_call" | custom-call | tf_op jit(solution)/shard_map/mixer_and_experts/pallas_call | solution.py:520
  87.0 1.5 %slice_bitcast_fusion = (bf16[256,128]{1,0:T(8,128)(2,1)}, bf16[256,128]{1,0:T(8,128)(2,1)}) fusion(bf16[2,256,128]{2,1,0:T(8,128)(2,1)} %mixer_and_experts.1), kind=kLoop, calls=%fused_computation | loop fusion | bytes 262144 | tf_op jit(solution)/shard_map/squeeze | solution.py:549
